TPU v7x, 32 devices: a whole 2x2x4 slice. The times are simulated.
32 devices in a mesh: ep: 8 (over z, y), tp: 4 (over x, core).
Axes of the slice: x: 2, y: 2, z: 4, core: 2. Of those that a mesh axis runs over, the one named last changes fastest.
Arguments:
- tokens: bfloat16 [512, 1024], P('ep', 'tp'), may hold values from -6 to 6
- conv_state: bfloat16 [512, 3, 512], P('ep', None, 'tp'), may hold values from -6 to 6
- lru_state: float32 [512, 512], P('ep', 'tp'), may hold values from -6 to 6
- mix_gain: bfloat16 [1024], replicated, may hold values from 0.099609375 to 1.8984375
- ffn_gain: bfloat16 [1024], replicated, may hold values from 0.099609375 to 1.8984375
- w_branch: bfloat16 [1024, 512], P(None, 'tp'), may hold values from -0.1875 to 0.1875
- w_gate: bfloat16 [1024, 512], P(None, 'tp'), may hold values from -0.1875 to 0.1875
- conv_taps: bfloat16 [4, 512], P(None, 'tp'), may hold values from -3 to 3
- w_recur: bfloat16 [8, 64, 64], P('tp'), may hold values from -0.75 to 0.75
- w_inject: bfloat16 [8, 64, 64], P('tp'), may hold values from -0.75 to 0.75
- lru_lambda: float32 [512], P('tp'), may hold values from 2 to 7
- w_out: bfloat16 [512, 1024], P('tp'), may hold values from -0.25 to 0.25
- expert_gate: bfloat16 [8, 1024, 2560], P('ep', None, 'tp'), may hold values from -0.1875 to 0.1875
- expert_up: bfloat16 [8, 1024, 2560], P('ep', None, 'tp'), may hold values from -0.1875 to 0.1875
- expert_down: bfloat16 [8, 2560, 1024], P('ep', 'tp'), may hold values from -0.125 to 0.125
- route_ids: int32 [512, 2], P('ep'), may hold values from 0 to 7, all different within a row; in each aligned block of 64 rows (0 to 63, 64 to 127, ...) at most 32 rows name the same one
- route_weight: float32 [512, 2], P('ep'), may hold values from 0.2 to 1
Outputs:
- mixed: bfloat16 [512, 1024], P('ep', 'tp')
- state_out: float32 [512, 512], P('ep', 'tp')
Inputs may be any that keep to these rules, and one draw needn't show every extreme that they name: `route_ids`: each row names 2 different experts. Among the 64 rows of one device no expert is named more than 32 times, and in every draw some expert is named exactly 32 times by them.
All inputs are finite; a program needn't handle non-finite values.
Results may differ from a plain program's by a relative error of at most 0.015.
Values may be sent and summed in bfloat16 or wider, within the bound.
No kernel may reach another device: no remote copies, remote signals or barrier semaphores. Data moves between devices by JAX's collectives and lax.ppermute only.
A program may use at most 64 MiB of HBM per device.

v0:
```python
import jax
import jax.numpy as jnp
import numpy as np
from jax import lax
from jax.experimental import pallas as pl
from jax.experimental.pallas import tpu as pltpu
from jax.sharding import Mesh, PartitionSpec as P

EPS = 1e-06
LRU_SCALE = 8.0
SWAP = ((0, 1), (1, 0))
F32, BF16 = jnp.float32, jnp.bfloat16


def call(kernel, outs, *args, scratch=(), flops=0, final=(), limit=4 << 20, far=0):
    away = tuple(pltpu.with_memory_space_constraint(a, pltpu.HBM) for a in args[:far])
    near = tuple(pltpu.with_memory_space_constraint(a, pltpu.VMEM) for a in args[far:])
    return pl.pallas_call(
        kernel,
        out_shape=[
            jax.ShapeDtypeStruct(s, d) if i in final else pltpu.VMEM(s, d)
            for i, (s, d) in enumerate(outs)
        ],
        in_specs=[pl.BlockSpec(memory_space=pltpu.HBM)] * far
        + [pl.BlockSpec(memory_space=pltpu.VMEM)] * len(near),
        out_specs=[pl.BlockSpec(memory_space=pltpu.VMEM)] * len(outs),
        scratch_shapes=list(scratch),
        compiler_params=pltpu.CompilerParams(vmem_limit_bytes=limit),
        cost_estimate=pl.CostEstimate(flops=flops, bytes_accessed=0, transcendentals=0),
    )(*away, *near)


def dot(a, b):
    return jnp.dot(a, b, preferred_element_type=F32)


def tp_index():
    return lax.axis_index("xa") * lax.axis_size("xb") + lax.axis_index("xb")


def span(i, size):
    return pl.ds(pl.multiple_of(i * size, size), size)


def pack(conv_h, taps_h, wr_h, wi_h, lam_h, state_h, tok_h, rows, tok, conv, taps, wr, wi, lam, sem):
    seqs, channels = state_h.shape
    held = (conv, taps, wr, wi, lam)
    targets = held + (rows.at[seqs : 2 * seqs, :], tok)
    sources = (conv_h, taps_h, wr_h, wi_h, lam_h, state_h, tok_h)
    copies = [
        pltpu.make_async_copy(h, v, sem.at[i]) for i, (h, v) in enumerate(zip(sources, targets))
    ]
    for c in copies:
        c.start()
    ends = 2 * seqs
    rows[ends:, :] = jnp.zeros((rows.shape[0] - ends, channels), F32)
    for c in copies[: len(held)]:
        c.wait()
    total = conv[0].astype(F32) * taps[0:1, :].astype(F32)
    for j in range(1, conv.shape[0]):
        total = total + conv[j].astype(F32) * taps[j : j + 1, :].astype(F32)
    rows[:seqs, :] = total
    rows[ends : ends + 1, :] = taps[conv.shape[0] :, :].astype(F32)
    rows[ends + 1 : ends + 2, :] = -LRU_SCALE * jnp.log1p(jnp.exp(-lam[...])).reshape(1, -1)
    heads, width = wr.shape[0], wr.shape[1]
    for i, w in enumerate((wr, wi)):
        base = ends + 8 + i * channels
        for h in range(heads):
            at = slice(h * width, (h + 1) * width)
            rows[base + h * width : base + (h + 1) * width, at] = w[h].astype(F32)
    for c in copies[len(held) :]:
        c.wait()
    base = ends + 8 + 2 * channels
    for i in range(tok.shape[1] // channels):
        at = slice(i * channels, (i + 1) * channels)
        rows[base + i * seqs : base + (i + 1) * seqs, :] = tok[:, at].astype(F32)


def prepare(mix_h, ffn_h, b_h, g_h, o_h, _, mix_row, ffn_row, b, g, o, mix_gain, ffn_gain, sem):
    pairs = ((mix_h, mix_gain), (ffn_h, ffn_gain), (b_h, b), (g_h, g), (o_h, o))
    copies = [pltpu.make_async_copy(h, v, sem.at[i]) for i, (h, v) in enumerate(pairs)]
    for c in copies:
        c.start()
    for c in copies[:2]:
        c.wait()
    mix_row[...] = mix_gain[...].astype(F32).reshape(mix_row.shape)
    ffn_row[...] = ffn_gain[...].astype(F32).reshape(ffn_row.shape)
    for c in copies[2:]:
        c.wait()


def pick(experts, half):
    def pick_kernel(ids_h, weight_h, _, named, hits, wcol, ids, weight, sem):
        copies = [
            pltpu.make_async_copy(h, v, sem.at[i])
            for i, (h, v) in enumerate(((ids_h, ids), (weight_h, weight)))
        ]
        for c in copies:
            c.start()
        top, seqs = ids.shape
        slots = named.shape[0]
        one, other = (lax.broadcasted_iota(jnp.int32, (seqs, seqs), i) for i in range(2))
        earlier = (one < other).astype(BF16)
        number = lax.broadcasted_iota(jnp.int32, (experts, seqs), 0)
        down = lax.broadcasted_iota(jnp.int32, (slots, seqs), 0).astype(F32)
        across = lax.broadcasted_iota(jnp.int32, (seqs, slots), 1).astype(F32)
        base = jnp.zeros((experts, 1), F32)
        sent = jnp.zeros((slots, seqs), F32)
        for c in copies:
            c.wait()
        for k in range(top):
            row = ids[k : k + 1, :]
            mine = (number == row).astype(F32)
            before = dot(mine.astype(BF16), earlier) + base
            slot = jnp.sum(before * mine, axis=0, keepdims=True)
            base = base + jnp.sum(mine, axis=1, keepdims=True)
            part = jnp.floor((slot + 0.5) * (1 / half))
            place = part * (experts * half) + row.astype(F32) * half + (slot - part * half)
            sent = sent + (down == place).astype(F32)
            column = jnp.sum(jnp.where(one == other, place, 0.0), axis=1, keepdims=True)
            hits[k * seqs : (k + 1) * seqs, :] = (across == column).astype(F32).astype(BF16)
            column = jnp.sum(
                jnp.where(one == other, weight[k : k + 1, :], 0.0), axis=1, keepdims=True
            )
            wcol[k] = jnp.broadcast_to(column, wcol.shape[1:])
        named[...] = sent.astype(BF16)

    return pick_kernel


def mixer(t0, t2, t3, mix_row, b0, b1, g0, g1, out0, out1, rows0, rows1, state_out, keep, give):
    me = tp_index()
    seqs, quarter = t0.shape
    channels = rows0.shape[1]
    base = 2 * seqs + 8 + 2 * channels
    t1 = jnp.concatenate([rows1[i : i + seqs, :] for i in range(base, rows1.shape[0], seqs)], axis=1)
    pieces = [t0[...].astype(F32), t1, t2[...].astype(F32), t3[...].astype(F32)]
    squares = sum(jnp.sum(p * p, axis=1, keepdims=True) for p in pieces)
    scale = lax.rsqrt(squares / (len(pieces) * quarter) + EPS)
    sums = [0.0] * 4
    for k, p in enumerate(pieces):
        at = span(me ^ k, quarter)
        normed = (p * scale * mix_row[:, at]).astype(BF16)
        sums = [v + dot(normed, w[at, :]) for v, w in zip(sums, (b0, g0, b1, g1))]
    kept = given = 0.0
    own, beside = span(me, quarter), span(me ^ 3, quarter)
    for i, (rows, w_out) in enumerate(((rows0, out0), (rows1, out1))):
        branch, gate_in = (v.astype(BF16).astype(F32) for v in sums[2 * i : 2 * i + 2])
        conv_out = rows[:seqs, :] + branch * rows[2 * seqs : 2 * seqs + 1, :]
        heads = conv_out.astype(BF16)
        maps = 2 * seqs + 8
        recur = jax.nn.sigmoid(dot(heads, rows[maps : maps + channels, :].astype(BF16)))
        inject = jax.nn.sigmoid(dot(heads, rows[maps + channels : maps + 2 * channels, :].astype(BF16)))
        log_decay = recur * rows[2 * seqs + 1 : 2 * seqs + 2, :]
        y = -2.0 * log_decay
        series = y * (1.0 - y * (1 / 2) * (1.0 - y * (1 / 3) * (1.0 - y * (1 / 4) * (1.0 - y * (1 / 5)))))
        left = jnp.where(y < 0.1, series, 1.0 - jnp.exp(-y))
        out = jnp.exp(log_decay) * rows[seqs : 2 * seqs, :] + jnp.sqrt(left) * inject * conv_out
        if i == 0:
            state_out[...] = out
        lru_out = (out * jax.nn.gelu(gate_in)).astype(BF16)
        kept = kept + dot(lru_out, w_out[:, own])
        given = given + dot(lru_out, w_out[:, beside])
    keep[...] = kept
    give[...] = given.astype(BF16)


def send_rows(tokens, keep, other, named, resid, sent):
    mix_out = (keep[...] + other[...].astype(F32)).astype(BF16).astype(F32)
    rows = (tokens[...].astype(F32) + mix_out).astype(BF16)
    resid[...] = rows
    slots = named.shape[0]
    buffer = dot(named[...], rows).astype(BF16)
    for a in range(0, sent.shape[0], slots):
        sent[a : a + slots, :] = buffer


def experts_of(got, ffn_row, g0, u0, d0, g1, u1, d1, out, rows):
    count, quarter = rows.shape[0], got.shape[1]
    squares = 0.0
    for a in range(0, got.shape[0], count):
        v = got[a : a + count, :].astype(F32)
        squares = squares + jnp.sum(v * v, axis=1, keepdims=True)
    scale = lax.rsqrt(squares / rows.shape[1] + EPS)
    for t in range(got.shape[0] // count):
        at = slice(t * quarter, (t + 1) * quarter)
        v = got[t * count : (t + 1) * count, :].astype(F32)
        rows[:, at] = (v * scale * ffn_row[:, at]).astype(BF16)
    term = 0.0
    for g, u, d in ((g0, u0, d0), (g1, u1, d1)):
        hidden = (jax.nn.silu(dot(rows[...], g[0])) * dot(rows[...], u[0])).astype(BF16)
        term = term + dot(hidden, d[0])
    for t in range(got.shape[0] // count):
        out[t * count : (t + 1) * count, :] = term[:, t * quarter : (t + 1) * quarter].astype(BF16)


def combine(resid, back, hits, wcol, mixed):
    top, seqs, width = wcol.shape
    slots = hits.shape[1]
    picked = sum(dot(hits[...], back[a : a + slots, :]) for a in range(0, back.shape[0], slots))
    for i in range(0, resid.shape[1], width):
        total = resid[:, i : i + width].astype(F32)
        for k in range(top):
            total = total + picked[k * seqs : (k + 1) * seqs, i : i + width] * wcol[k]
        mixed[:, i : i + width] = total.astype(BF16)


def step(
    tokens,
    conv_state,
    lru_state,
    mix_gain,
    ffn_gain,
    w_branch,
    w_gate,
    conv_taps,
    w_recur,
    w_inject,
    lru_lambda,
    w_out,
    expert_gate,
    expert_up,
    expert_down,
    route_ids,
    route_weight,
):
    seqs, quarter = tokens.shape
    top = route_ids.shape[1]
    channels = lru_state.shape[1]
    tp = ("xa", "xb")
    na = lax.axis_size("xa")
    n_tp = na * lax.axis_size("xb")
    features = n_tp * quarter
    experts = lax.axis_size("ep") * expert_gate.shape[0]
    nb = lax.axis_size("xb")
    capacity = max(2, 2 * seqs * top // experts)
    half = -(-capacity // nb)
    slots = nb * experts * half
    ring = ("xa", "xb", "ep")

    def swapped(x, k):
        return lax.ppermute(x, tp, [(i, i ^ k) for i in range(n_tp)])

    others = [swapped(tokens, k) for k in range(2, n_tp)]

    def beside(x):
        return lax.ppermute(x, "xb", SWAP)

    b_1, g_1, out_1 = (beside(w) for w in (w_branch, w_gate, w_out))
    mixing = (
        conv_state.transpose(1, 0, 2),
        conv_taps,
        w_recur,
        w_inject,
        lru_lambda,
        lru_state,
        tokens,
    )
    rows_0, here = call(
        pack,
        [
            ((2 * seqs + 8 + 2 * channels + seqs * (quarter // channels), channels), F32),
            (tokens.shape, BF16),
        ],
        *mixing,
        far=len(mixing),
        scratch=[pltpu.VMEM(a.shape, a.dtype) for a in mixing[:5]]
        + [pltpu.SemaphoreType.DMA((len(mixing),))],
        flops=10**5,
    )
    rows_1 = beside(rows_0)
    large = (w_branch, w_gate, w_out)
    mix_row, ffn_row, b_0, g_0, out_0 = call(
        prepare,
        [((1, features), F32)] * 2 + [(a.shape, a.dtype) for a in large],
        mix_gain,
        ffn_gain,
        *large,
        rows_0,
        far=2 + len(large),
        scratch=[pltpu.VMEM(a.shape, a.dtype) for a in (mix_gain, ffn_gain)]
        + [pltpu.SemaphoreType.DMA((2 + len(large),))],
        flops=10**6,
    )
    state_out, keep, give = call(
        mixer,
        [((seqs, channels), F32), ((seqs, quarter), F32), ((seqs, quarter), BF16)],
        here,
        *others,
        mix_row,
        b_0,
        b_1,
        g_0,
        g_1,
        out_0,
        out_1,
        rows_0,
        rows_1,
        flops=10**8,
        final=(0,),
    )
    routes = (route_ids.T, route_weight.T)
    named, hits, wcol = call(
        pick(experts, half),
        [((slots, seqs), BF16), ((top * seqs, slots), BF16), ((top, seqs, 128), F32)],
        *routes,
        keep,
        far=2,
        scratch=[pltpu.VMEM(a.shape, a.dtype) for a in routes] + [pltpu.SemaphoreType.DMA((2,))],
        flops=10**6,
    )
    resid, sent = call(
        send_rows,
        [((seqs, quarter), BF16), ((na * slots, quarter), BF16)],
        here,
        keep,
        swapped(give, 3),
        named,
        flops=10**7,
    )
    partners = []
    for w in (expert_gate, expert_up, expert_down):
        partners.append(lax.ppermute(w, "xb", SWAP))
    arrived = lax.all_to_all(sent, ring, split_axis=0, concat_axis=0, tiled=True)
    (term,) = call(
        experts_of,
        [((na * slots, quarter), BF16)],
        arrived,
        ffn_row,
        expert_gate,
        expert_up,
        expert_down,
        *partners,
        scratch=[pltpu.VMEM((slots // nb, features), BF16)],
        flops=10**9,
        limit=8 << 20,
    )
    back = lax.all_to_all(term, ring, split_axis=0, concat_axis=0, tiled=True)
    (mixed,) = call(combine, [((seqs, quarter), BF16)], resid, back, hits, wcol, final=(0,))
    return (mixed, state_out)


def solution(mesh):
    n_ep, n_tp = mesh.shape["ep"], mesh.shape["tp"]
    finer = Mesh(np.asarray(mesh.devices).reshape(n_ep, n_tp // 2, 2), ("ep", "xa", "xb"))
    tp = ("xa", "xb")
    placed = (
        P("ep", tp),
        P("ep", None, tp),
        P("ep", tp),
        P(),
        P(),
        P(None, tp),
        P(None, tp),
        P(None, tp),
        P(tp, None, None),
        P(tp, None, None),
        P(tp),
        P(tp, None),
        P("ep", None, tp),
        P("ep", None, tp),
        P("ep", tp, None),
        P("ep", None),
        P("ep", None),
    )
    return jax.shard_map(step, mesh=finer, in_specs=placed, out_specs=(P("ep", tp), P("ep", tp)), check_vma=False)
```

profile of v0, /device:TPU:0, one launch (start us, length us, event | category | flops | bytes accessed | tf_op | source)
XLA Modules:
  0.0 47.8 jit_solution(8200391040783565619)
XLA Ops:
  0.6 0.6 %collective-permute-start.7 = (bf16[1,1024,640]{2,1,0:T(8,128)(2,1)}, bf16[1,1024,640]{2,1,0:T(8,128)(2,1)S(1)}, u32[]{:S(2)}, u32[]{:S(2)}) collective-permute-start(bf16[1,1024,640]{2,1,0:T(8,128)(2,1)} %g0.1), channel_id=1, source_target_pairs={{0,1},{1,0},{2,3},{3,2},{4,5},{5,4},{6,7},{7,6},{8,9},{9,8},{10,11... | collective-permute-start | bytes 3932168 | tf_op jit(solution)/shard_map/ppermute | solution.py:323
  1.2 0.1 collective-permute-start.8
  1.3 0.4 collective-permute-start.9
  1.7 2.6 %collective-permute-start.1 = (bf16[64,256]{1,0:T(8,128)(2,1)}, bf16[64,256]{1,0:T(8,128)(2,1)S(1)}, u32[]{:S(2)}, u32[]{:S(2)}) collective-permute-start(bf16[64,256]{1,0:T(8,128)(2,1)} %tok_h.1), channel_id=1, source_target_pairs={{0,3},{1,2},{2,1},{3,0},{4,7},{5,6},{6,5},{7,4},{8,11},{9,10},{10,... | collective-permute-start | bytes 98312 | tf_op jit(solution)/shard_map/ppermute | solution.py:242
  4.3 0.0 collective-permute-start
  4.3 1.9 %collective-permute-done.1.t3 = bf16[64,256]{1,0:T(8,128)(2,1)S(1)} collective-permute-done((bf16[64,256]{1,0:T(8,128)(2,1)}, bf16[64,256]{1,0:T(8,128)(2,1)S(1)}, u32[]{:S(2)}, u32[]{:S(2)}) %collective-permute-start.1) | collective-permute-done | bytes 32800 | tf_op jit(solution)/shard_map/ppermute | solution.py:242
  6.2 0.1 collective-permute-start.2
  6.3 2.1 %collective-permute-done.t2 = bf16[64,256]{1,0:T(8,128)(2,1)S(1)} collective-permute-done((bf16[64,256]{1,0:T(8,128)(2,1)}, bf16[64,256]{1,0:T(8,128)(2,1)S(1)}, u32[]{:S(2)}, u32[]{:S(2)}) %collective-permute-start) | collective-permute-done | bytes 32800 | tf_op jit(solution)/shard_map/ppermute | solution.py:242
  8.4 0.0 collective-permute-start.3
  8.4 1.0 %shard_map.176 = (f32[520,128]{1,0:T(8,128)S(1)}, bf16[64,256]{1,0:T(8,128)(2,1)S(1)}) custom-call(bf16[3,64,128]{2,1,0:T(8,128)(2,1)} %bitcast.11, bf16[4,128]{1,0:T(4,128)(2,1)} %taps_h.1, bf16[2,64,64]{2,1,0:T(8,128)(2,1)} %wr_h.1, bf16[2,64,64]{2,1,0:T(8,128)(2,1)} %wi_h.1, f32[128]{0:T(128)} %lam_h.1, f32[64,128]{1,0:T(8,128)} %state_h.1, ...), custom_call_target="tpu_custom_call" | custom-call | flops 100000 | tf_op jit(solution)/shard_map/pallas_call | solution.py:18
  9.4 0.0 collective-permute-done.2.b1
  9.4 0.6 %collective-permute-start.5 = (f32[520,128]{1,0:T(8,128)S(1)}, f32[520,128]{1,0:T(8,128)S(1)}, u32[]{:S(2)}, u32[]{:S(2)}) collective-permute-start(f32[520,128]{1,0:T(8,128)S(1)} %get-tuple-element.18._.rows0), channel_id=1, source_target_pairs={{0,1},{1,0},{2,3},{3,2},{4,5},{5,4},{6,7},{7,6},{8,9},{9,8},{10,11... | collective-permute-start | bytes 798728 | tf_op jit(solution)/shard_map/ppermute | solution.py:247
  10.0 0.2 collective-permute-done.3.g1
  10.2 0.1 collective-permute-start.4
  10.3 0.0 copy-start.2
  10.3 1.3 %shard_map.177 = (f32[1,1024]{1,0:T(1,128)S(1)}, f32[1,1024]{1,0:T(1,128)S(1)}, bf16[1024,128]{1,0:T(8,128)(2,1)S(1)}, bf16[1024,128]{1,0:T(8,128)(2,1)S(1)}, bf16[128,1024]{1,0:T(8,128)(2,1)S(1)}) custom-call(bf16[1024]{0:T(1024)(128)(2,1)} %mix_h.1, bf16[1024]{0:T(1024)(128)(2,1)} %ffn_h.1, bf16[1024,128]{1,0:T(8,128)(2,1)} %b_h.1, bf16[1024,128]{1,0:T(8,128)(2,1)} %g_h.1, ...), custom_call_target="tpu_custom_call" | custom-call | flops 1000000 | tf_op jit(solution)/shard_map/pallas_call | solution.py:18
  11.6 0.3 collective-permute-done.4.out1
  11.9 0.0 collective-permute-done.5.rows1
  11.9 0.0 copy-start
  11.9 0.0 copy-start.1
  11.9 1.2 %shard_map.178 = (f32[64,128]{1,0:T(8,128)}, f32[64,256]{1,0:T(8,128)S(1)}, bf16[64,256]{1,0:T(8,128)(2,1)S(1)}) custom-call(bf16[64,256]{1,0:T(8,128)(2,1)S(1)} %get-tuple-element.17.t0.tokens, bf16[64,256]{1,0:T(8,128)(2,1)S(1)} %collective-permute-done.t2, bf16[64,256]{1,0:T(8,128)(2,1)S(1)} %collective-permute-done.1.t3, ...), custom_call_target="tpu_custom_call" | custom-call | flops 100000000 | tf_op jit(solution)/shard_map/pallas_call | solution.py:18
  13.1 1.0 %collective-permute-start.6 = (bf16[64,256]{1,0:T(8,128)(2,1)S(1)}, bf16[64,256]{1,0:T(8,128)(2,1)S(1)}, u32[]{:S(2)}, u32[]{:S(2)}) collective-permute-start(bf16[64,256]{1,0:T(8,128)(2,1)S(1)} %get-tuple-element.24), channel_id=1, source_target_pairs={{0,3},{1,2},{2,1},{3,0},{4,7},{5,6},{6,5},{7,4},{8,11},{9,10},{10,... | collective-permute-start | bytes 98312 | tf_op jit(solution)/shard_map/ppermute | solution.py:242
  14.1 1.0 %shard_map.179 = (bf16[256,64]{1,0:T(8,128)(2,1)S(1)}, bf16[128,256]{1,0:T(8,128)(2,1)S(1)}, f32[2,64,128]{2,1,0:T(8,128)S(1)}) custom-call(s32[2,64]{1,0:T(2,128)} %bitcast.12, f32[2,64]{1,0:T(2,128)} %bitcast.13, f32[64,256]{1,0:T(8,128)S(1)} %get-tuple-element.23._.keep), custom_call_target="tpu_custom_call" | custom-call | flops 1000000 | tf_op jit(solution)/shard_map/pallas_call | solution.py:18
  15.1 1.4 %collective-permute-done.6.other = bf16[64,256]{1,0:T(8,128)(2,1)S(1)} collective-permute-done((bf16[64,256]{1,0:T(8,128)(2,1)S(1)}, bf16[64,256]{1,0:T(8,128)(2,1)S(1)}, u32[]{:S(2)}, u32[]{:S(2)}) %collective-permute-start.6) | collective-permute-done | bytes 32800 | tf_op jit(solution)/shard_map/ppermute | solution.py:242
  16.5 0.2 shard_map.180
  16.7 15.8 %all_to_all.22 = bf16[32,16,256]{2,1,0:T(8,128)(2,1)S(1)} all-to-all(bf16[32,16,256]{2,1,0:T(8,128)(2,1)S(1)} %bitcast.10), channel_id=1, replica_groups=mesh['ep'=8,'xa'=2,'xb'=2] {'xa','xb','ep'}, dimensions={0} | all-to-all | bytes 524288 | tf_op jit(solution)/shard_map/all_to_all | solution.py:324
  32.5 0.0 collective-permute-done.7.g1
  32.5 0.0 collective-permute-done.8.u1
  32.5 0.0 collective-permute-done.9.d1
  32.6 0.0 copy-done.2
  32.6 0.0 copy-done
  32.6 0.0 copy-done.1
  32.6 1.6 %shard_map.181 = bf16[512,256]{1,0:T(8,128)(2,1)S(1)} custom-call(bf16[512,256]{1,0:T(8,128)(2,1)S(1)} %bitcast.8, f32[1,1024]{1,0:T(1,128)S(1)} %get-tuple-element.28.ffn_row, bf16[1,1024,640]{2,1,0:T(8,128)(2,1)S(1)} %copy-done, bf16[1,1024,640]{2,1,0:T(8,128)(2,1)S(1)} %copy-done.1, bf16[1,640,1024]{2,1,0:T(8,128)(2,1)S(1)} %copy-done.2, ...), custom_call_target="tpu_custom_call" | custom-call | flops 1000000000 | tf_op jit(solution)/shard_map/pallas_call | solution.py:18
  34.2 12.8 %all_to_all.23 = bf16[32,16,256]{2,1,0:T(8,128)(2,1)S(1)} all-to-all(bf16[32,16,256]{2,1,0:T(8,128)(2,1)S(1)} %bitcast.9), channel_id=1, replica_groups=mesh['ep'=8,'xa'=2,'xb'=2] {'xa','xb','ep'}, dimensions={0} | all-to-all | bytes 524288 | tf_op jit(solution)/shard_map/all_to_all | solution.py:338
  47.0 0.8 %shard_map.182 = bf16[64,256]{1,0:T(8,128)(2,1)} custom-call(bf16[64,256]{1,0:T(8,128)(2,1)S(1)} %get-tuple-element.26.resid, bf16[512,256]{1,0:T(8,128)(2,1)S(1)} %bitcast.7, bf16[128,256]{1,0:T(8,128)(2,1)S(1)} %get-tuple-element.29.hits, f32[2,64,128]{2,1,0:T(8,128)S(1)} %get-tuple-element.30.wcol), custom_call_target="tpu_custom_call" | custom-call | tf_op jit(solution)/shard_map/pallas_call | solution.py:18
Async XLA Ops:
  0.6 31.9 %collective-permute-start.7 = (bf16[1,1024,640]{2,1,0:T(8,128)(2,1)}, bf16[1,1024,640]{2,1,0:T(8,128)(2,1)S(1)}, u32[]{:S(2)}, u32[]{:S(2)}) collective-permute-start(bf16[1,1024,640]{2,1,0:T(8,128)(2,1)} %g0.1), channel_id=1, source_target_pairs={{0,1},{1,0},{2,3},{3,2},{4,5},{5,4},{6,7},{7,6},{8,9},{9,8},{10,11... | collective-permute-start | bytes 3932168 | tf_op jit(solution)/shard_map/ppermute | solution.py:323
  1.2 31.4 %collective-permute-start.8 = (bf16[1,1024,640]{2,1,0:T(8,128)(2,1)}, bf16[1,1024,640]{2,1,0:T(8,128)(2,1)S(1)}, u32[]{:S(2)}, u32[]{:S(2)}) collective-permute-start(bf16[1,1024,640]{2,1,0:T(8,128)(2,1)} %u0.1), channel_id=1, source_target_pairs={{0,1},{1,0},{2,3},{3,2},{4,5},{5,4},{6,7},{7,6},{8,9},{9,8},{10,11... | collective-permute-start | bytes 3932168 | tf_op jit(solution)/shard_map/ppermute | solution.py:323
  1.3 31.3 %collective-permute-start.9 = (bf16[1,640,1024]{2,1,0:T(8,128)(2,1)}, bf16[1,640,1024]{2,1,0:T(8,128)(2,1)S(1)}, u32[]{:S(2)}, u32[]{:S(2)}) collective-permute-start(bf16[1,640,1024]{2,1,0:T(8,128)(2,1)} %d0.1), channel_id=1, source_target_pairs={{0,1},{1,0},{2,3},{3,2},{4,5},{5,4},{6,7},{7,6},{8,9},{9,8},{10,11... | collective-permute-start | bytes 3932168 | tf_op jit(solution)/shard_map/ppermute | solution.py:323
  1.7 4.5 %collective-permute-start.1 = (bf16[64,256]{1,0:T(8,128)(2,1)}, bf16[64,256]{1,0:T(8,128)(2,1)S(1)}, u32[]{:S(2)}, u32[]{:S(2)}) collective-permute-start(bf16[64,256]{1,0:T(8,128)(2,1)} %tok_h.1), channel_id=1, source_target_pairs={{0,3},{1,2},{2,1},{3,0},{4,7},{5,6},{6,5},{7,4},{8,11},{9,10},{10,... | collective-permute-start | bytes 98312 | tf_op jit(solution)/shard_map/ppermute | solution.py:242
  4.3 4.1 %collective-permute-start = (bf16[64,256]{1,0:T(8,128)(2,1)}, bf16[64,256]{1,0:T(8,128)(2,1)S(1)}, u32[]{:S(2)}, u32[]{:S(2)}) collective-permute-start(bf16[64,256]{1,0:T(8,128)(2,1)} %tok_h.1), channel_id=1, source_target_pairs={{0,2},{1,3},{2,0},{3,1},{4,6},{5,7},{6,4},{7,5},{8,10},{9,11},{10,... | collective-permute-start | bytes 98312 | tf_op jit(solution)/shard_map/ppermute | solution.py:242
  6.2 3.2 %collective-permute-start.2 = (bf16[1024,128]{1,0:T(8,128)(2,1)}, bf16[1024,128]{1,0:T(8,128)(2,1)S(1)}, u32[]{:S(2)}, u32[]{:S(2)}) collective-permute-start(bf16[1024,128]{1,0:T(8,128)(2,1)} %b_h.1), channel_id=1, source_target_pairs={{0,1},{1,0},{2,3},{3,2},{4,5},{5,4},{6,7},{7,6},{8,9},{9,8},{10,11... | collective-permute-start | bytes 786440 | tf_op jit(solution)/shard_map/ppermute | solution.py:247
  8.4 1.7 %collective-permute-start.3 = (bf16[1024,128]{1,0:T(8,128)(2,1)}, bf16[1024,128]{1,0:T(8,128)(2,1)S(1)}, u32[]{:S(2)}, u32[]{:S(2)}) collective-permute-start(bf16[1024,128]{1,0:T(8,128)(2,1)} %g_h.1), channel_id=1, source_target_pairs={{0,1},{1,0},{2,3},{3,2},{4,5},{5,4},{6,7},{7,6},{8,9},{9,8},{10,11... | collective-permute-start | bytes 786440 | tf_op jit(solution)/shard_map/ppermute | solution.py:247
  9.4 2.5 %collective-permute-start.5 = (f32[520,128]{1,0:T(8,128)S(1)}, f32[520,128]{1,0:T(8,128)S(1)}, u32[]{:S(2)}, u32[]{:S(2)}) collective-permute-start(f32[520,128]{1,0:T(8,128)S(1)} %get-tuple-element.18._.rows0), channel_id=1, source_target_pairs={{0,1},{1,0},{2,3},{3,2},{4,5},{5,4},{6,7},{7,6},{8,9},{9,8},{10,11... | collective-permute-start | bytes 798728 | tf_op jit(solution)/shard_map/ppermute | solution.py:247
  10.2 1.7 %collective-permute-start.4 = (bf16[128,1024]{1,0:T(8,128)(2,1)}, bf16[128,1024]{1,0:T(8,128)(2,1)S(1)}, u32[]{:S(2)}, u32[]{:S(2)}) collective-permute-start(bf16[128,1024]{1,0:T(8,128)(2,1)} %o_h.1), channel_id=1, source_target_pairs={{0,1},{1,0},{2,3},{3,2},{4,5},{5,4},{6,7},{7,6},{8,9},{9,8},{10,11... | collective-permute-start | bytes 786440 | tf_op jit(solution)/shard_map/ppermute | solution.py:247
  10.3 22.3 %copy-start.2 = (bf16[1,640,1024]{2,1,0:T(8,128)(2,1)S(1)}, bf16[1,640,1024]{2,1,0:T(8,128)(2,1)}, u32[]{:S(2)}) copy-start(bf16[1,640,1024]{2,1,0:T(8,128)(2,1)} %d0.1) | copy-start | bytes 3932164
  11.9 20.7 %copy-start = (bf16[1,1024,640]{2,1,0:T(8,128)(2,1)S(1)}, bf16[1,1024,640]{2,1,0:T(8,128)(2,1)}, u32[]{:S(2)}) copy-start(bf16[1,1024,640]{2,1,0:T(8,128)(2,1)} %g0.1) | copy-start | bytes 3932164
  11.9 20.7 %copy-start.1 = (bf16[1,1024,640]{2,1,0:T(8,128)(2,1)S(1)}, bf16[1,1024,640]{2,1,0:T(8,128)(2,1)}, u32[]{:S(2)}) copy-start(bf16[1,1024,640]{2,1,0:T(8,128)(2,1)} %u0.1) | copy-start | bytes 3932164
  13.1 3.4 %collective-permute-start.6 = (bf16[64,256]{1,0:T(8,128)(2,1)S(1)}, bf16[64,256]{1,0:T(8,128)(2,1)S(1)}, u32[]{:S(2)}, u32[]{:S(2)}) collective-permute-start(bf16[64,256]{1,0:T(8,128)(2,1)S(1)} %get-tuple-element.24), channel_id=1, source_target_pairs={{0,3},{1,2},{2,1},{3,0},{4,7},{5,6},{6,5},{7,4},{8,11},{9,10},{10,... | collective-permute-start | bytes 98312 | tf_op jit(solution)/shard_map/ppermute | solution.py:242
where the time goes:
time: 48 us; the launch traced here: 47.8 us
  blocking collectives  28.6 us (60%)
  Pallas kernels  7.03 us (15%)
  waiting for transfers between devices  5.93 us (12%)
  starting transfers between devices  5.46 us (11%)
  between operations  0.72 us (2%)
    all_to_all x1, blocking collectives, step(): lax.all_to_all(sent, ring, split_axis=0, concat_axis=0, tiled=True)  15.8 us
    all_to_all x1, blocking collectives, step(): back = lax.all_to_all(term, ring, split_axis=0, concat_axis=0, tiled=True)  12.8 us
    pallas_call x7, Pallas kernels, call(): pl.pallas_call(kernel, out_shape=[jax.ShapeDtypeStruct(s, d) if i in fina...  7.03 us
    ppermute x3, waiting for transfers between devices, swapped(): return lax.ppermute(x, tp, [(i, i ^ k) for i in range(n_tp)])  5.42 us
    ppermute x3, starting transfers between devices, swapped(): return lax.ppermute(x, tp, [(i, i ^ k) for i in range(n_tp)])  3.58 us
    ppermute x3, starting transfers between devices, step(): partners.append(lax.ppermute(w, 'xb', SWAP))  1.07 us
  transfers between devices with their start and end apart: 10, of which 5 were waited for; matrix products, arithmetic and copies ran while one was open for 0% of the time, Pallas kernels for 10%

commit v1 on v0

--- a/solution.py
+++ b/solution.py
@@ -23,7 +23,9 @@
         ],
         in_specs=[pl.BlockSpec(memory_space=pltpu.HBM)] * far
         + [pl.BlockSpec(memory_space=pltpu.VMEM)] * len(near),
-        out_specs=[pl.BlockSpec(memory_space=pltpu.VMEM)] * len(outs),
+        out_specs=[
+            pl.BlockSpec(memory_space=pl.ANY if i in final else pltpu.VMEM) for i in range(len(outs))
+        ],
         scratch_shapes=list(scratch),
         compiler_params=pltpu.CompilerParams(vmem_limit_bytes=limit),
         cost_estimate=pl.CostEstimate(flops=flops, bytes_accessed=0, transcendentals=0),
@@ -178,31 +180,36 @@
 def experts_of(got, ffn_row, g0, u0, d0, g1, u1, d1, out, rows):
     count, quarter = rows.shape[0], got.shape[1]
     squares = 0.0
-    for a in range(0, got.shape[0], count):
-        v = got[a : a + count, :].astype(F32)
-        squares = squares + jnp.sum(v * v, axis=1, keepdims=True)
-    scale = lax.rsqrt(squares / rows.shape[1] + EPS)
     for t in range(got.shape[0] // count):
         at = slice(t * quarter, (t + 1) * quarter)
         v = got[t * count : (t + 1) * count, :].astype(F32)
-        rows[:, at] = (v * scale * ffn_row[:, at]).astype(BF16)
+        rows[:, at] = (v * ffn_row[:, at]).astype(BF16)
+        squares = squares + jnp.sum(v * v, axis=1, keepdims=True)
+    scale = lax.rsqrt(squares / rows.shape[1] + EPS)
     term = 0.0
     for g, u, d in ((g0, u0, d0), (g1, u1, d1)):
-        hidden = (jax.nn.silu(dot(rows[...], g[0])) * dot(rows[...], u[0])).astype(BF16)
-        term = term + dot(hidden, d[0])
+        first, second = dot(rows[...], g[0]) * scale, dot(rows[...], u[0]) * scale
+        term = term + dot((jax.nn.silu(first) * second).astype(BF16), d[0])
     for t in range(got.shape[0] // count):
         out[t * count : (t + 1) * count, :] = term[:, t * quarter : (t + 1) * quarter].astype(BF16)
 
 
-def combine(resid, back, hits, wcol, mixed):
+def combine(resid, back, hits, wcol, state, mixed_h, state_h, mixed, sem):
+    leaving = [pltpu.make_async_copy(state, state_h, sem.at[0])]
+    leaving[0].start()
     top, seqs, width = wcol.shape
     slots = hits.shape[1]
-    picked = sum(dot(hits[...], back[a : a + slots, :]) for a in range(0, back.shape[0], slots))
-    for i in range(0, resid.shape[1], width):
-        total = resid[:, i : i + width].astype(F32)
+    for j, i in enumerate(range(0, resid.shape[1], width)):
+        at = slice(i, i + width)
+        picked = sum(dot(hits[...], back[a : a + slots, at]) for a in range(0, back.shape[0], slots))
+        total = resid[:, at].astype(F32)
         for k in range(top):
-            total = total + picked[k * seqs : (k + 1) * seqs, i : i + width] * wcol[k]
-        mixed[:, i : i + width] = total.astype(BF16)
+            total = total + picked[k * seqs : (k + 1) * seqs, :] * wcol[k]
+        mixed[:, at] = total.astype(BF16)
+        leaving.append(pltpu.make_async_copy(mixed.at[:, at], mixed_h.at[:, at], sem.at[j + 1]))
+        leaving[-1].start()
+    for c in leaving:
+        c.wait()
 
 
 def step(
@@ -282,7 +289,7 @@
         + [pltpu.SemaphoreType.DMA((2 + len(large),))],
         flops=10**6,
     )
-    state_out, keep, give = call(
+    state, keep, give = call(
         mixer,
         [((seqs, channels), F32), ((seqs, quarter), F32), ((seqs, quarter), BF16)],
         here,
@@ -297,7 +304,6 @@
         rows_0,
         rows_1,
         flops=10**8,
-        final=(0,),
     )
     routes = (route_ids.T, route_weight.T)
     named, hits, wcol = call(
@@ -336,8 +342,17 @@
         limit=8 << 20,
     )
     back = lax.all_to_all(term, ring, split_axis=0, concat_axis=0, tiled=True)
-    (mixed,) = call(combine, [((seqs, quarter), BF16)], resid, back, hits, wcol, final=(0,))
-    return (mixed, state_out)
+    return call(
+        combine,
+        [((seqs, quarter), BF16), ((seqs, channels), F32)],
+        resid,
+        back,
+        hits,
+        wcol,
+        state,
+        final=(0, 1),
+        scratch=[pltpu.VMEM((seqs, quarter), BF16), pltpu.SemaphoreType.DMA((1 + quarter // 128,))],
+    )
 
 
 def solution(mesh):

time: 48 us -> 47.6 us (level)
  Pallas kernels: 7.03 us -> 6.53 us
    pallas_call x7, Pallas kernels: 7.03 us -> 6.53 us  [call(): pl.pallas_call(kernel, out_shape=[jax.ShapeDtypeStruct(s, d) if i in fina...]
  transfers between devices with their start and end apart: 10 -> 10, of which waited for: 5 -> 5; matrix products, arithmetic and copies ran while one was open for 0% -> 0% of each run, Pallas kernels for 10% -> 9%
where the time goes in v1:
time: 47.6 us; the launch traced here: 47.4 us
  blocking collectives  28.6 us (60%)
  Pallas kernels  6.53 us (14%)
  waiting for transfers between devices  5.93 us (12%)
  starting transfers between devices  5.52 us (12%)
  between operations  0.73 us (2%)
    all_to_all x1, blocking collectives, step(): lax.all_to_all(sent, ring, split_axis=0, concat_axis=0, tiled=True)  15.8 us
    all_to_all x1, blocking collectives, step(): back = lax.all_to_all(term, ring, split_axis=0, concat_axis=0, tiled=True)  12.8 us
    pallas_call x7, Pallas kernels, call(): pl.pallas_call(kernel, out_shape=[jax.ShapeDtypeStruct(s, d) if i in fina...  6.53 us
    ppermute x3, waiting for transfers between devices, swapped(): return lax.ppermute(x, tp, [(i, i ^ k) for i in range(n_tp)])  5.42 us
    ppermute x3, starting transfers between devices, swapped(): return lax.ppermute(x, tp, [(i, i ^ k) for i in range(n_tp)])  3.65 us
    ppermute x3, starting transfers between devices, step(): partners.append(lax.ppermute(w, 'xb', SWAP))  1.07 us
  transfers between devices with their start and end apart: 10, of which 5 were waited for; matrix products, arithmetic and copies ran while one was open for 0% of the time, Pallas kernels for 9%

profile of v1, /device:TPU:0, one launch (start us, length us, event | category | flops | bytes accessed | tf_op | source)
XLA Modules:
  0.0 47.4 jit_solution(4735873917123421047)
XLA Ops:
  0.6 0.6 %collective-permute-start.7 = (bf16[1,1024,640]{2,1,0:T(8,128)(2,1)}, bf16[1,1024,640]{2,1,0:T(8,128)(2,1)S(1)}, u32[]{:S(2)}, u32[]{:S(2)}) collective-permute-start(bf16[1,1024,640]{2,1,0:T(8,128)(2,1)} %g0.1), channel_id=1, source_target_pairs={{0,1},{1,0},{2,3},{3,2},{4,5},{5,4},{6,7},{7,6},{8,9},{9,8},{10,11... | collective-permute-start | bytes 3932168 | tf_op jit(solution)/shard_map/ppermute | solution.py:329
  1.2 0.1 collective-permute-start.8
  1.3 0.4 collective-permute-start.9
  1.7 2.6 %collective-permute-start.1 = (bf16[64,256]{1,0:T(8,128)(2,1)}, bf16[64,256]{1,0:T(8,128)(2,1)S(1)}, u32[]{:S(2)}, u32[]{:S(2)}) collective-permute-start(bf16[64,256]{1,0:T(8,128)(2,1)} %tok_h.1), channel_id=1, source_target_pairs={{0,3},{1,2},{2,1},{3,0},{4,7},{5,6},{6,5},{7,4},{8,11},{9,10},{10,... | collective-permute-start | bytes 98312 | tf_op jit(solution)/shard_map/ppermute | solution.py:249
  4.3 0.0 collective-permute-start
  4.3 1.9 %collective-permute-done.1.t3 = bf16[64,256]{1,0:T(8,128)(2,1)S(1)} collective-permute-done((bf16[64,256]{1,0:T(8,128)(2,1)}, bf16[64,256]{1,0:T(8,128)(2,1)S(1)}, u32[]{:S(2)}, u32[]{:S(2)}) %collective-permute-start.1) | collective-permute-done | bytes 32800 | tf_op jit(solution)/shard_map/ppermute | solution.py:249
  6.2 0.1 collective-permute-start.2
  6.3 2.1 %collective-permute-done.t2 = bf16[64,256]{1,0:T(8,128)(2,1)S(1)} collective-permute-done((bf16[64,256]{1,0:T(8,128)(2,1)}, bf16[64,256]{1,0:T(8,128)(2,1)S(1)}, u32[]{:S(2)}, u32[]{:S(2)}) %collective-permute-start) | collective-permute-done | bytes 32800 | tf_op jit(solution)/shard_map/ppermute | solution.py:249
  8.4 0.0 collective-permute-start.3
  8.4 1.0 %shard_map.176 = (f32[520,128]{1,0:T(8,128)S(1)}, bf16[64,256]{1,0:T(8,128)(2,1)S(1)}) custom-call(bf16[3,64,128]{2,1,0:T(8,128)(2,1)} %bitcast.11, bf16[4,128]{1,0:T(4,128)(2,1)} %taps_h.1, bf16[2,64,64]{2,1,0:T(8,128)(2,1)} %wr_h.1, bf16[2,64,64]{2,1,0:T(8,128)(2,1)} %wi_h.1, f32[128]{0:T(128)} %lam_h.1, f32[64,128]{1,0:T(8,128)} %state_h.1, ...), custom_call_target="tpu_custom_call" | custom-call | flops 100000 | tf_op jit(solution)/shard_map/pallas_call | solution.py:18
  9.4 0.0 collective-permute-done.2.b1
  9.4 0.6 %collective-permute-start.5 = (f32[520,128]{1,0:T(8,128)S(1)}, f32[520,128]{1,0:T(8,128)S(1)}, u32[]{:S(2)}, u32[]{:S(2)}) collective-permute-start(f32[520,128]{1,0:T(8,128)S(1)} %get-tuple-element.18._.rows0), channel_id=1, source_target_pairs={{0,1},{1,0},{2,3},{3,2},{4,5},{5,4},{6,7},{7,6},{8,9},{9,8},{10,11... | collective-permute-start | bytes 798728 | tf_op jit(solution)/shard_map/ppermute | solution.py:254
  10.0 0.2 collective-permute-done.3.g1
  10.2 0.1 collective-permute-start.4
  10.3 0.0 copy-start.2
  10.3 1.3 %shard_map.177 = (f32[1,1024]{1,0:T(1,128)S(1)}, f32[1,1024]{1,0:T(1,128)S(1)}, bf16[1024,128]{1,0:T(8,128)(2,1)S(1)}, bf16[1024,128]{1,0:T(8,128)(2,1)S(1)}, bf16[128,1024]{1,0:T(8,128)(2,1)S(1)}) custom-call(bf16[1024]{0:T(1024)(128)(2,1)} %mix_h.1, bf16[1024]{0:T(1024)(128)(2,1)} %ffn_h.1, bf16[1024,128]{1,0:T(8,128)(2,1)} %b_h.1, bf16[1024,128]{1,0:T(8,128)(2,1)} %g_h.1, ...), custom_call_target="tpu_custom_call" | custom-call | flops 1000000 | tf_op jit(solution)/shard_map/pallas_call | solution.py:18
  11.6 0.3 collective-permute-done.4.out1
  11.9 0.0 collective-permute-done.5.rows1
  11.9 0.0 copy-start
  11.9 0.0 copy-start.1
  11.9 0.7 %shard_map.178 = (f32[64,128]{1,0:T(8,128)S(1)}, f32[64,256]{1,0:T(8,128)S(1)}, bf16[64,256]{1,0:T(8,128)(2,1)S(1)}) custom-call(bf16[64,256]{1,0:T(8,128)(2,1)S(1)} %get-tuple-element.17.t0.tokens, bf16[64,256]{1,0:T(8,128)(2,1)S(1)} %collective-permute-done.t2, bf16[64,256]{1,0:T(8,128)(2,1)S(1)} %collective-permute-done.1.t3, ...), custom_call_target="tpu_custom_call" | custom-call | flops 100000000 | tf_op jit(solution)/shard_map/pallas_call | solution.py:18
  12.7 1.1 %collective-permute-start.6 = (bf16[64,256]{1,0:T(8,128)(2,1)S(1)}, bf16[64,256]{1,0:T(8,128)(2,1)S(1)}, u32[]{:S(2)}, u32[]{:S(2)}) collective-permute-start(bf16[64,256]{1,0:T(8,128)(2,1)S(1)} %get-tuple-element.24), channel_id=1, source_target_pairs={{0,3},{1,2},{2,1},{3,0},{4,7},{5,6},{6,5},{7,4},{8,11},{9,10},{10,... | collective-permute-start | bytes 98312 | tf_op jit(solution)/shard_map/ppermute | solution.py:249
  13.7 1.0 %shard_map.179 = (bf16[256,64]{1,0:T(8,128)(2,1)S(1)}, bf16[128,256]{1,0:T(8,128)(2,1)S(1)}, f32[2,64,128]{2,1,0:T(8,128)S(1)}) custom-call(s32[2,64]{1,0:T(2,128)} %bitcast.12, f32[2,64]{1,0:T(2,128)} %bitcast.13, f32[64,256]{1,0:T(8,128)S(1)} %get-tuple-element.23._.keep), custom_call_target="tpu_custom_call" | custom-call | flops 1000000 | tf_op jit(solution)/shard_map/pallas_call | solution.py:18
  14.7 1.4 %collective-permute-done.6.other = bf16[64,256]{1,0:T(8,128)(2,1)S(1)} collective-permute-done((bf16[64,256]{1,0:T(8,128)(2,1)S(1)}, bf16[64,256]{1,0:T(8,128)(2,1)S(1)}, u32[]{:S(2)}, u32[]{:S(2)}) %collective-permute-start.6) | collective-permute-done | bytes 32800 | tf_op jit(solution)/shard_map/ppermute | solution.py:249
  16.1 0.2 shard_map.180
  16.3 15.8 %all_to_all.22 = bf16[32,16,256]{2,1,0:T(8,128)(2,1)S(1)} all-to-all(bf16[32,16,256]{2,1,0:T(8,128)(2,1)S(1)} %bitcast.10), channel_id=1, replica_groups=mesh['ep'=8,'xa'=2,'xb'=2] {'xa','xb','ep'}, dimensions={0} | all-to-all | bytes 524288 | tf_op jit(solution)/shard_map/all_to_all | solution.py:330
  32.1 0.0 collective-permute-done.7.g1
  32.1 0.0 collective-permute-done.8.u1
  32.1 0.0 collective-permute-done.9.d1
  32.1 0.0 copy-done.2
  32.2 0.0 copy-done
  32.2 0.0 copy-done.1
  32.2 1.5 %shard_map.181 = bf16[512,256]{1,0:T(8,128)(2,1)S(1)} custom-call(bf16[512,256]{1,0:T(8,128)(2,1)S(1)} %bitcast.8, f32[1,1024]{1,0:T(1,128)S(1)} %get-tuple-element.28.ffn_row, bf16[1,1024,640]{2,1,0:T(8,128)(2,1)S(1)} %copy-done, bf16[1,1024,640]{2,1,0:T(8,128)(2,1)S(1)} %copy-done.1, bf16[1,640,1024]{2,1,0:T(8,128)(2,1)S(1)} %copy-done.2, ...), custom_call_target="tpu_custom_call" | custom-call | flops 1000000000 | tf_op jit(solution)/shard_map/pallas_call | solution.py:18
  33.7 12.8 %all_to_all.23 = bf16[32,16,256]{2,1,0:T(8,128)(2,1)S(1)} all-to-all(bf16[32,16,256]{2,1,0:T(8,128)(2,1)S(1)} %bitcast.9), channel_id=1, replica_groups=mesh['ep'=8,'xa'=2,'xb'=2] {'xa','xb','ep'}, dimensions={0} | all-to-all | bytes 524288 | tf_op jit(solution)/shard_map/all_to_all | solution.py:344
  46.5 0.9 %shard_map.182 = (bf16[64,256]{1,0:T(8,128)(2,1)}, f32[64,128]{1,0:T(8,128)}) custom-call(bf16[64,256]{1,0:T(8,128)(2,1)S(1)} %get-tuple-element.26.resid, bf16[512,256]{1,0:T(8,128)(2,1)S(1)} %bitcast.7, bf16[128,256]{1,0:T(8,128)(2,1)S(1)} %get-tuple-element.29.hits, f32[2,64,128]{2,1,0:T(8,128)S(1)} %get-tuple-element.30.wcol, ...), custom_call_target="tpu_custom_call" | custom-call | tf_op jit(solution)/shard_map/pallas_call | solution.py:18
Async XLA Ops:
  0.6 31.5 %collective-permute-start.7 = (bf16[1,1024,640]{2,1,0:T(8,128)(2,1)}, bf16[1,1024,640]{2,1,0:T(8,128)(2,1)S(1)}, u32[]{:S(2)}, u32[]{:S(2)}) collective-permute-start(bf16[1,1024,640]{2,1,0:T(8,128)(2,1)} %g0.1), channel_id=1, source_target_pairs={{0,1},{1,0},{2,3},{3,2},{4,5},{5,4},{6,7},{7,6},{8,9},{9,8},{10,11... | collective-permute-start | bytes 3932168 | tf_op jit(solution)/shard_map/ppermute | solution.py:329
  1.2 30.9 %collective-permute-start.8 = (bf16[1,1024,640]{2,1,0:T(8,128)(2,1)}, bf16[1,1024,640]{2,1,0:T(8,128)(2,1)S(1)}, u32[]{:S(2)}, u32[]{:S(2)}) collective-permute-start(bf16[1,1024,640]{2,1,0:T(8,128)(2,1)} %u0.1), channel_id=1, source_target_pairs={{0,1},{1,0},{2,3},{3,2},{4,5},{5,4},{6,7},{7,6},{8,9},{9,8},{10,11... | collective-permute-start | bytes 3932168 | tf_op jit(solution)/shard_map/ppermute | solution.py:329
  1.3 30.9 %collective-permute-start.9 = (bf16[1,640,1024]{2,1,0:T(8,128)(2,1)}, bf16[1,640,1024]{2,1,0:T(8,128)(2,1)S(1)}, u32[]{:S(2)}, u32[]{:S(2)}) collective-permute-start(bf16[1,640,1024]{2,1,0:T(8,128)(2,1)} %d0.1), channel_id=1, source_target_pairs={{0,1},{1,0},{2,3},{3,2},{4,5},{5,4},{6,7},{7,6},{8,9},{9,8},{10,11... | collective-permute-start | bytes 3932168 | tf_op jit(solution)/shard_map/ppermute | solution.py:329
  1.7 4.5 %collective-permute-start.1 = (bf16[64,256]{1,0:T(8,128)(2,1)}, bf16[64,256]{1,0:T(8,128)(2,1)S(1)}, u32[]{:S(2)}, u32[]{:S(2)}) collective-permute-start(bf16[64,256]{1,0:T(8,128)(2,1)} %tok_h.1), channel_id=1, source_target_pairs={{0,3},{1,2},{2,1},{3,0},{4,7},{5,6},{6,5},{7,4},{8,11},{9,10},{10,... | collective-permute-start | bytes 98312 | tf_op jit(solution)/shard_map/ppermute | solution.py:249
  4.3 4.1 %collective-permute-start = (bf16[64,256]{1,0:T(8,128)(2,1)}, bf16[64,256]{1,0:T(8,128)(2,1)S(1)}, u32[]{:S(2)}, u32[]{:S(2)}) collective-permute-start(bf16[64,256]{1,0:T(8,128)(2,1)} %tok_h.1), channel_id=1, source_target_pairs={{0,2},{1,3},{2,0},{3,1},{4,6},{5,7},{6,4},{7,5},{8,10},{9,11},{10,... | collective-permute-start | bytes 98312 | tf_op jit(solution)/shard_map/ppermute | solution.py:249
  6.2 3.2 %collective-permute-start.2 = (bf16[1024,128]{1,0:T(8,128)(2,1)}, bf16[1024,128]{1,0:T(8,128)(2,1)S(1)}, u32[]{:S(2)}, u32[]{:S(2)}) collective-permute-start(bf16[1024,128]{1,0:T(8,128)(2,1)} %b_h.1), channel_id=1, source_target_pairs={{0,1},{1,0},{2,3},{3,2},{4,5},{5,4},{6,7},{7,6},{8,9},{9,8},{10,11... | collective-permute-start | bytes 786440 | tf_op jit(solution)/shard_map/ppermute | solution.py:254
  8.4 1.7 %collective-permute-start.3 = (bf16[1024,128]{1,0:T(8,128)(2,1)}, bf16[1024,128]{1,0:T(8,128)(2,1)S(1)}, u32[]{:S(2)}, u32[]{:S(2)}) collective-permute-start(bf16[1024,128]{1,0:T(8,128)(2,1)} %g_h.1), channel_id=1, source_target_pairs={{0,1},{1,0},{2,3},{3,2},{4,5},{5,4},{6,7},{7,6},{8,9},{9,8},{10,11... | collective-permute-start | bytes 786440 | tf_op jit(solution)/shard_map/ppermute | solution.py:254
  9.4 2.5 %collective-permute-start.5 = (f32[520,128]{1,0:T(8,128)S(1)}, f32[520,128]{1,0:T(8,128)S(1)}, u32[]{:S(2)}, u32[]{:S(2)}) collective-permute-start(f32[520,128]{1,0:T(8,128)S(1)} %get-tuple-element.18._.rows0), channel_id=1, source_target_pairs={{0,1},{1,0},{2,3},{3,2},{4,5},{5,4},{6,7},{7,6},{8,9},{9,8},{10,11... | collective-permute-start | bytes 798728 | tf_op jit(solution)/shard_map/ppermute | solution.py:254
  10.2 1.7 %collective-permute-start.4 = (bf16[128,1024]{1,0:T(8,128)(2,1)}, bf16[128,1024]{1,0:T(8,128)(2,1)S(1)}, u32[]{:S(2)}, u32[]{:S(2)}) collective-permute-start(bf16[128,1024]{1,0:T(8,128)(2,1)} %o_h.1), channel_id=1, source_target_pairs={{0,1},{1,0},{2,3},{3,2},{4,5},{5,4},{6,7},{7,6},{8,9},{9,8},{10,11... | collective-permute-start | bytes 786440 | tf_op jit(solution)/shard_map/ppermute | solution.py:254
  10.3 21.8 %copy-start.2 = (bf16[1,640,1024]{2,1,0:T(8,128)(2,1)S(1)}, bf16[1,640,1024]{2,1,0:T(8,128)(2,1)}, u32[]{:S(2)}) copy-start(bf16[1,640,1024]{2,1,0:T(8,128)(2,1)} %d0.1) | copy-start | bytes 3932164
  11.9 20.2 %copy-start = (bf16[1,1024,640]{2,1,0:T(8,128)(2,1)S(1)}, bf16[1,1024,640]{2,1,0:T(8,128)(2,1)}, u32[]{:S(2)}) copy-start(bf16[1,1024,640]{2,1,0:T(8,128)(2,1)} %g0.1) | copy-start | bytes 3932164
  11.9 20.3 %copy-start.1 = (bf16[1,1024,640]{2,1,0:T(8,128)(2,1)S(1)}, bf16[1,1024,640]{2,1,0:T(8,128)(2,1)}, u32[]{:S(2)}) copy-start(bf16[1,1024,640]{2,1,0:T(8,128)(2,1)} %u0.1) | copy-start | bytes 3932164
  12.7 3.4 %collective-permute-start.6 = (bf16[64,256]{1,0:T(8,128)(2,1)S(1)}, bf16[64,256]{1,0:T(8,128)(2,1)S(1)}, u32[]{:S(2)}, u32[]{:S(2)}) collective-permute-start(bf16[64,256]{1,0:T(8,128)(2,1)S(1)} %get-tuple-element.24), channel_id=1, source_target_pairs={{0,3},{1,2},{2,1},{3,0},{4,7},{5,6},{6,5},{7,4},{8,11},{9,10},{10,... | collective-permute-start | bytes 98312 | tf_op jit(solution)/shard_map/ppermute | solution.py:249

commit v2 on v1

--- a/solution.py
+++ b/solution.py
@@ -91,7 +91,7 @@
         c.wait()
 
 
-def pick(experts, half):
+def pick(experts, capacity):
     def pick_kernel(ids_h, weight_h, _, named, hits, wcol, ids, weight, sem):
         copies = [
             pltpu.make_async_copy(h, v, sem.at[i])
@@ -116,8 +116,7 @@
             before = dot(mine.astype(BF16), earlier) + base
             slot = jnp.sum(before * mine, axis=0, keepdims=True)
             base = base + jnp.sum(mine, axis=1, keepdims=True)
-            part = jnp.floor((slot + 0.5) * (1 / half))
-            place = part * (experts * half) + row.astype(F32) * half + (slot - part * half)
+            place = row.astype(F32) * capacity + slot
             sent = sent + (down == place).astype(F32)
             column = jnp.sum(jnp.where(one == other, place, 0.0), axis=1, keepdims=True)
             hits[k * seqs : (k + 1) * seqs, :] = (across == column).astype(F32).astype(BF16)
@@ -178,20 +177,25 @@
 
 
 def experts_of(got, ffn_row, g0, u0, d0, g1, u1, d1, out, rows):
-    count, quarter = rows.shape[0], got.shape[1]
+    na, sources, both, quarter = got.shape
+    nb = rows.shape[1] // (na * quarter)
+    half = both // nb
+    blocks = [(x, slice(c * half, (c + 1) * half)) for x in range(na) for c in range(nb)]
     squares = 0.0
-    for t in range(got.shape[0] // count):
+    for t, (x, part) in enumerate(blocks):
         at = slice(t * quarter, (t + 1) * quarter)
-        v = got[t * count : (t + 1) * count, :].astype(F32)
+        v = got[x, :, part, :].reshape(sources * half, quarter).astype(F32)
         rows[:, at] = (v * ffn_row[:, at]).astype(BF16)
         squares = squares + jnp.sum(v * v, axis=1, keepdims=True)
     scale = lax.rsqrt(squares / rows.shape[1] + EPS)
-    term = 0.0
-    for g, u, d in ((g0, u0, d0), (g1, u1, d1)):
+    hidden = []
+    for g, u in ((g0, u0), (g1, u1)):
         first, second = dot(rows[...], g[0]) * scale, dot(rows[...], u[0]) * scale
-        term = term + dot((jax.nn.silu(first) * second).astype(BF16), d[0])
-    for t in range(got.shape[0] // count):
-        out[t * count : (t + 1) * count, :] = term[:, t * quarter : (t + 1) * quarter].astype(BF16)
+        hidden.append((jax.nn.silu(first) * second).astype(BF16))
+    for t, (x, part) in enumerate(blocks):
+        at = slice(t * quarter, (t + 1) * quarter)
+        term = dot(hidden[0], d0[0, :, at]) + dot(hidden[1], d1[0, :, at])
+        out[x, :, part, :] = term.astype(BF16).reshape(sources, half, quarter)
 
 
 def combine(resid, back, hits, wcol, state, mixed_h, state_h, mixed, sem):
@@ -243,7 +247,7 @@
     capacity = max(2, 2 * seqs * top // experts)
     half = -(-capacity // nb)
     slots = nb * experts * half
-    ring = ("xa", "xb", "ep")
+    ring = ("xa", "ep", "xb")
 
     def swapped(x, k):
         return lax.ppermute(x, tp, [(i, i ^ k) for i in range(n_tp)])
@@ -303,11 +307,11 @@
         out_1,
         rows_0,
         rows_1,
-        flops=10**8,
+        flops=5*10**9,
     )
     routes = (route_ids.T, route_weight.T)
     named, hits, wcol = call(
-        pick(experts, half),
+        pick(experts, nb * half),
         [((slots, seqs), BF16), ((top * seqs, slots), BF16), ((top, seqs, 128), F32)],
         *routes,
         keep,
@@ -327,11 +331,12 @@
     partners = []
     for w in (expert_gate, expert_up, expert_down):
         partners.append(lax.ppermute(w, "xb", SWAP))
+    blocks = (na, experts, nb * half, quarter)
     arrived = lax.all_to_all(sent, ring, split_axis=0, concat_axis=0, tiled=True)
     (term,) = call(
         experts_of,
-        [((na * slots, quarter), BF16)],
-        arrived,
+        [(blocks, BF16)],
+        arrived.reshape(blocks),
         ffn_row,
         expert_gate,
         expert_up,
@@ -341,7 +346,7 @@
         flops=10**9,
         limit=8 << 20,
     )
-    back = lax.all_to_all(term, ring, split_axis=0, concat_axis=0, tiled=True)
+    back = lax.all_to_all(term.reshape(na * slots, quarter), ring, split_axis=0, concat_axis=0, tiled=True)
     return call(
         combine,
         [((seqs, quarter), BF16), ((seqs, channels), F32)],

time: 47.6 us -> 47.7 us (level)
  starting transfers between devices: 5.52 us -> 6.18 us
    ppermute x3, waiting for transfers between devices: 5.42 us -> 4.3 us  [swapped(): return lax.ppermute(x, tp, [(i, i ^ k) for i in range(n_tp)])]
    ppermute x3, starting transfers between devices: 3.65 us -> 4.62 us  [swapped(): return lax.ppermute(x, tp, [(i, i ^ k) for i in range(n_tp)])]
    ppermute x3, starting transfers between devices: 1.07 us -> 0.26 us  [step(): partners.append(lax.ppermute(w, 'xb', SWAP))]
    ppermute x4, waiting for transfers between devices: 0.5 us -> 1.16 us  [beside(): return lax.ppermute(x, 'xb', SWAP)]
    ppermute x4, starting transfers between devices: 0.81 us -> 1.3 us  [beside(): return lax.ppermute(x, 'xb', SWAP)]
  transfers between devices with their start and end apart: 10 -> 10, of which waited for: 5 -> 4; matrix products, arithmetic and copies ran while one was open for 0% -> 0% of each run, Pallas kernels for 9% -> 9%
where the time goes in v2:
time: 47.7 us; the launch traced here: 47.5 us
  blocking collectives  28.7 us (60%)
  Pallas kernels  6.41 us (13%)
  starting transfers between devices  6.18 us (13%)
  waiting for transfers between devices  5.47 us (11%)
  between operations  0.73 us (2%)
    all_to_all x1, blocking collectives, step(): lax.all_to_all(sent, ring, split_axis=0, concat_axis=0, tiled=True)  16.1 us
    all_to_all x1, blocking collectives, step(): lax.all_to_all(term.reshape(na * slots, quarter), ring, split_axis=0, con...  12.6 us
    pallas_call x7, Pallas kernels, call(): pl.pallas_call(kernel, out_shape=[jax.ShapeDtypeStruct(s, d) if i in fina...  6.41 us
    ppermute x3, starting transfers between devices, swapped(): return lax.ppermute(x, tp, [(i, i ^ k) for i in range(n_tp)])  4.62 us
    ppermute x3, waiting for transfers between devices, swapped(): return lax.ppermute(x, tp, [(i, i ^ k) for i in range(n_tp)])  4.3 us
    ppermute x4, starting transfers between devices, beside(): return lax.ppermute(x, 'xb', SWAP)  1.3 us
    ppermute x4, waiting for transfers between devices, beside(): return lax.ppermute(x, 'xb', SWAP)  1.16 us
  transfers between devices with their start and end apart: 10, of which 4 were waited for; matrix products, arithmetic and copies ran while one was open for 0% of the time, Pallas kernels for 9%

profile of v2, /device:TPU:0, one launch (start us, length us, event | category | flops | bytes accessed | tf_op | source)
XLA Modules:
  0.0 47.5 jit_solution(17688241219455012997)
XLA Ops:
  0.6 0.6 %collective-permute-start.2 = (bf16[1024,128]{1,0:T(8,128)(2,1)}, bf16[1024,128]{1,0:T(8,128)(2,1)S(1)}, u32[]{:S(2)}, u32[]{:S(2)}) collective-permute-start(bf16[1024,128]{1,0:T(8,128)(2,1)} %b_h.1), channel_id=1, source_target_pairs={{0,1},{1,0},{2,3},{3,2},{4,5},{5,4},{6,7},{7,6},{8,9},{9,8},{10,11... | collective-permute-start | bytes 786440 | tf_op jit(solution)/shard_map/ppermute | solution.py:258
  1.2 0.1 collective-permute-start.3
  1.3 2.6 %collective-permute-start.1 = (bf16[64,256]{1,0:T(8,128)(2,1)}, bf16[64,256]{1,0:T(8,128)(2,1)S(1)}, u32[]{:S(2)}, u32[]{:S(2)}) collective-permute-start(bf16[64,256]{1,0:T(8,128)(2,1)} %tok_h.1), channel_id=1, source_target_pairs={{0,3},{1,2},{2,1},{3,0},{4,7},{5,6},{6,5},{7,4},{8,11},{9,10},{10,... | collective-permute-start | bytes 98312 | tf_op jit(solution)/shard_map/ppermute | solution.py:253
  3.9 0.3 collective-permute-start
  4.2 0.1 collective-permute-start.7
  4.3 1.7 %collective-permute-done.1.t3 = bf16[64,256]{1,0:T(8,128)(2,1)S(1)} collective-permute-done((bf16[64,256]{1,0:T(8,128)(2,1)}, bf16[64,256]{1,0:T(8,128)(2,1)S(1)}, u32[]{:S(2)}, u32[]{:S(2)}) %collective-permute-start.1) | collective-permute-done | bytes 32800 | tf_op jit(solution)/shard_map/ppermute | solution.py:253
  6.0 0.1 collective-permute-start.8
  6.1 1.9 %collective-permute-done.t2 = bf16[64,256]{1,0:T(8,128)(2,1)S(1)} collective-permute-done((bf16[64,256]{1,0:T(8,128)(2,1)}, bf16[64,256]{1,0:T(8,128)(2,1)S(1)}, u32[]{:S(2)}, u32[]{:S(2)}) %collective-permute-start) | collective-permute-done | bytes 32800 | tf_op jit(solution)/shard_map/ppermute | solution.py:253
  8.0 0.0 collective-permute-start.9
  8.0 1.0 %shard_map.176 = (f32[520,128]{1,0:T(8,128)S(1)}, bf16[64,256]{1,0:T(8,128)(2,1)S(1)}) custom-call(bf16[3,64,128]{2,1,0:T(8,128)(2,1)} %bitcast.11, bf16[4,128]{1,0:T(4,128)(2,1)} %taps_h.1, bf16[2,64,64]{2,1,0:T(8,128)(2,1)} %wr_h.1, bf16[2,64,64]{2,1,0:T(8,128)(2,1)} %wi_h.1, f32[128]{0:T(128)} %lam_h.1, f32[64,128]{1,0:T(8,128)} %state_h.1, ...), custom_call_target="tpu_custom_call" | custom-call | flops 100000 | tf_op jit(solution)/shard_map/pallas_call | solution.py:18
  9.0 0.0 collective-permute-done.2.b1
  9.0 0.6 %collective-permute-start.5 = (f32[520,128]{1,0:T(8,128)S(1)}, f32[520,128]{1,0:T(8,128)S(1)}, u32[]{:S(2)}, u32[]{:S(2)}) collective-permute-start(f32[520,128]{1,0:T(8,128)S(1)} %get-tuple-element.18._.rows0), channel_id=1, source_target_pairs={{0,1},{1,0},{2,3},{3,2},{4,5},{5,4},{6,7},{7,6},{8,9},{9,8},{10,11... | collective-permute-start | bytes 798728 | tf_op jit(solution)/shard_map/ppermute | solution.py:258
  9.6 0.0 collective-permute-done.3.g1
  9.6 0.1 collective-permute-start.4
  9.6 1.2 %shard_map.177 = (f32[1,1024]{1,0:T(1,128)S(1)}, f32[1,1024]{1,0:T(1,128)S(1)}, bf16[1024,128]{1,0:T(8,128)(2,1)S(1)}, bf16[1024,128]{1,0:T(8,128)(2,1)S(1)}, bf16[128,1024]{1,0:T(8,128)(2,1)S(1)}) custom-call(bf16[1024]{0:T(1024)(128)(2,1)} %mix_h.1, bf16[1024]{0:T(1024)(128)(2,1)} %ffn_h.1, bf16[1024,128]{1,0:T(8,128)(2,1)} %b_h.1, bf16[1024,128]{1,0:T(8,128)(2,1)} %g_h.1, ...), custom_call_target="tpu_custom_call" | custom-call | flops 1000000 | tf_op jit(solution)/shard_map/pallas_call | solution.py:18
  10.8 1.2 %collective-permute-done.4.out1 = bf16[128,1024]{1,0:T(8,128)(2,1)S(1)} collective-permute-done((bf16[128,1024]{1,0:T(8,128)(2,1)}, bf16[128,1024]{1,0:T(8,128)(2,1)S(1)}, u32[]{:S(2)}, u32[]{:S(2)}) %collective-permute-start.4) | collective-permute-done | bytes 262176 | tf_op jit(solution)/shard_map/ppermute | solution.py:258
  12.0 0.0 collective-permute-done.5.rows1
  12.0 0.0 copy-start
  12.0 0.0 copy-start.1
  12.0 0.0 copy-start.2
  12.0 0.7 %shard_map.178 = (f32[64,128]{1,0:T(8,128)S(1)}, f32[64,256]{1,0:T(8,128)S(1)}, bf16[64,256]{1,0:T(8,128)(2,1)S(1)}) custom-call(bf16[64,256]{1,0:T(8,128)(2,1)S(1)} %get-tuple-element.17.t0.tokens, bf16[64,256]{1,0:T(8,128)(2,1)S(1)} %collective-permute-done.t2, bf16[64,256]{1,0:T(8,128)(2,1)S(1)} %collective-permute-done.1.t3, ...), custom_call_target="tpu_custom_call" | custom-call | flops 5000000000 | tf_op jit(solution)/shard_map/pallas_call | solution.py:18
  12.8 1.7 %collective-permute-start.6 = (bf16[64,256]{1,0:T(8,128)(2,1)S(1)}, bf16[64,256]{1,0:T(8,128)(2,1)S(1)}, u32[]{:S(2)}, u32[]{:S(2)}) collective-permute-start(bf16[64,256]{1,0:T(8,128)(2,1)S(1)} %get-tuple-element.24), channel_id=1, source_target_pairs={{0,3},{1,2},{2,1},{3,0},{4,7},{5,6},{6,5},{7,4},{8,11},{9,10},{10,... | collective-permute-start | bytes 98312 | tf_op jit(solution)/shard_map/ppermute | solution.py:253
  14.5 1.0 %shard_map.179 = (bf16[256,64]{1,0:T(8,128)(2,1)S(1)}, bf16[128,256]{1,0:T(8,128)(2,1)S(1)}, f32[2,64,128]{2,1,0:T(8,128)S(1)}) custom-call(s32[2,64]{1,0:T(2,128)} %bitcast.12, f32[2,64]{1,0:T(2,128)} %bitcast.13, f32[64,256]{1,0:T(8,128)S(1)} %get-tuple-element.23._.keep), custom_call_target="tpu_custom_call" | custom-call | flops 1000000 | tf_op jit(solution)/shard_map/pallas_call | solution.py:18
  15.4 0.7 %collective-permute-done.6.other = bf16[64,256]{1,0:T(8,128)(2,1)S(1)} collective-permute-done((bf16[64,256]{1,0:T(8,128)(2,1)S(1)}, bf16[64,256]{1,0:T(8,128)(2,1)S(1)}, u32[]{:S(2)}, u32[]{:S(2)}) %collective-permute-start.6) | collective-permute-done | bytes 32800 | tf_op jit(solution)/shard_map/ppermute | solution.py:253
  16.2 0.2 shard_map.180
  16.4 16.1 %all_to_all.20 = bf16[32,16,256]{2,1,0:T(8,128)(2,1)S(1)} all-to-all(bf16[32,16,256]{2,1,0:T(8,128)(2,1)S(1)} %bitcast.10), channel_id=1, replica_groups=mesh['ep'=8,'xa'=2,'xb'=2] {'xa','ep','xb'}, dimensions={0} | all-to-all | bytes 524288 | tf_op jit(solution)/shard_map/all_to_all | solution.py:335
  32.5 0.0 collective-permute-done.7.g1
  32.5 0.0 collective-permute-done.8.u1
  32.5 0.0 collective-permute-done.9.d1
  32.5 0.0 copy-done
  32.5 0.0 copy-done.1
  32.5 0.0 copy-done.2
  32.5 1.5 %shard_map.181 = bf16[2,8,32,256]{3,2,1,0:T(8,128)(2,1)S(1)} custom-call(bf16[2,8,32,256]{3,2,1,0:T(8,128)(2,1)S(1)} %bitcast.8, f32[1,1024]{1,0:T(1,128)S(1)} %get-tuple-element.28.ffn_row, bf16[1,1024,640]{2,1,0:T(8,128)(2,1)S(1)} %copy-done, bf16[1,1024,640]{2,1,0:T(8,128)(2,1)S(1)} %copy-done.1, bf16[1,640,1024]{2,1,0:T(8,128)(2,1)S(1)} %copy-done.2, ...), custom_call_target="tpu_custom_call" | custom-call | flops 1000000000 | tf_op jit(solution)/shard_map/pallas_call | solution.py:18
  34.0 12.6 %all_to_all.21 = bf16[32,16,256]{2,1,0:T(8,128)(2,1)S(1)} all-to-all(bf16[32,16,256]{2,1,0:T(8,128)(2,1)S(1)} %bitcast.9), channel_id=1, replica_groups=mesh['ep'=8,'xa'=2,'xb'=2] {'xa','ep','xb'}, dimensions={0} | all-to-all | bytes 524288 | tf_op jit(solution)/shard_map/all_to_all | solution.py:349
  46.6 0.9 %shard_map.182 = (bf16[64,256]{1,0:T(8,128)(2,1)}, f32[64,128]{1,0:T(8,128)}) custom-call(bf16[64,256]{1,0:T(8,128)(2,1)S(1)} %get-tuple-element.26.resid, bf16[512,256]{1,0:T(8,128)(2,1)S(1)} %bitcast.7, bf16[128,256]{1,0:T(8,128)(2,1)S(1)} %get-tuple-element.29.hits, f32[2,64,128]{2,1,0:T(8,128)S(1)} %get-tuple-element.30.wcol, ...), custom_call_target="tpu_custom_call" | custom-call | tf_op jit(solution)/shard_map/pallas_call | solution.py:18
Async XLA Ops:
  0.6 8.3 %collective-permute-start.2 = (bf16[1024,128]{1,0:T(8,128)(2,1)}, bf16[1024,128]{1,0:T(8,128)(2,1)S(1)}, u32[]{:S(2)}, u32[]{:S(2)}) collective-permute-start(bf16[1024,128]{1,0:T(8,128)(2,1)} %b_h.1), channel_id=1, source_target_pairs={{0,1},{1,0},{2,3},{3,2},{4,5},{5,4},{6,7},{7,6},{8,9},{9,8},{10,11... | collective-permute-start | bytes 786440 | tf_op jit(solution)/shard_map/ppermute | solution.py:258
  1.2 8.4 %collective-permute-start.3 = (bf16[1024,128]{1,0:T(8,128)(2,1)}, bf16[1024,128]{1,0:T(8,128)(2,1)S(1)}, u32[]{:S(2)}, u32[]{:S(2)}) collective-permute-start(bf16[1024,128]{1,0:T(8,128)(2,1)} %g_h.1), channel_id=1, source_target_pairs={{0,1},{1,0},{2,3},{3,2},{4,5},{5,4},{6,7},{7,6},{8,9},{9,8},{10,11... | collective-permute-start | bytes 786440 | tf_op jit(solution)/shard_map/ppermute | solution.py:258
  1.3 4.7 %collective-permute-start.1 = (bf16[64,256]{1,0:T(8,128)(2,1)}, bf16[64,256]{1,0:T(8,128)(2,1)S(1)}, u32[]{:S(2)}, u32[]{:S(2)}) collective-permute-start(bf16[64,256]{1,0:T(8,128)(2,1)} %tok_h.1), channel_id=1, source_target_pairs={{0,3},{1,2},{2,1},{3,0},{4,7},{5,6},{6,5},{7,4},{8,11},{9,10},{10,... | collective-permute-start | bytes 98312 | tf_op jit(solution)/shard_map/ppermute | solution.py:253
  3.9 4.1 %collective-permute-start = (bf16[64,256]{1,0:T(8,128)(2,1)}, bf16[64,256]{1,0:T(8,128)(2,1)S(1)}, u32[]{:S(2)}, u32[]{:S(2)}) collective-permute-start(bf16[64,256]{1,0:T(8,128)(2,1)} %tok_h.1), channel_id=1, source_target_pairs={{0,2},{1,3},{2,0},{3,1},{4,6},{5,7},{6,4},{7,5},{8,10},{9,11},{10,... | collective-permute-start | bytes 98312 | tf_op jit(solution)/shard_map/ppermute | solution.py:253
  4.2 28.3 %collective-permute-start.7 = (bf16[1,1024,640]{2,1,0:T(8,128)(2,1)}, bf16[1,1024,640]{2,1,0:T(8,128)(2,1)S(1)}, u32[]{:S(2)}, u32[]{:S(2)}) collective-permute-start(bf16[1,1024,640]{2,1,0:T(8,128)(2,1)} %g0.1), channel_id=1, source_target_pairs={{0,1},{1,0},{2,3},{3,2},{4,5},{5,4},{6,7},{7,6},{8,9},{9,8},{10,11... | collective-permute-start | bytes 3932168 | tf_op jit(solution)/shard_map/ppermute | solution.py:333
  6.0 26.5 %collective-permute-start.8 = (bf16[1,1024,640]{2,1,0:T(8,128)(2,1)}, bf16[1,1024,640]{2,1,0:T(8,128)(2,1)S(1)}, u32[]{:S(2)}, u32[]{:S(2)}) collective-permute-start(bf16[1,1024,640]{2,1,0:T(8,128)(2,1)} %u0.1), channel_id=1, source_target_pairs={{0,1},{1,0},{2,3},{3,2},{4,5},{5,4},{6,7},{7,6},{8,9},{9,8},{10,11... | collective-permute-start | bytes 3932168 | tf_op jit(solution)/shard_map/ppermute | solution.py:333
  8.0 24.5 %collective-permute-start.9 = (bf16[1,640,1024]{2,1,0:T(8,128)(2,1)}, bf16[1,640,1024]{2,1,0:T(8,128)(2,1)S(1)}, u32[]{:S(2)}, u32[]{:S(2)}) collective-permute-start(bf16[1,640,1024]{2,1,0:T(8,128)(2,1)} %d0.1), channel_id=1, source_target_pairs={{0,1},{1,0},{2,3},{3,2},{4,5},{5,4},{6,7},{7,6},{8,9},{9,8},{10,11... | collective-permute-start | bytes 3932168 | tf_op jit(solution)/shard_map/ppermute | solution.py:333
  9.0 3.0 %collective-permute-start.5 = (f32[520,128]{1,0:T(8,128)S(1)}, f32[520,128]{1,0:T(8,128)S(1)}, u32[]{:S(2)}, u32[]{:S(2)}) collective-permute-start(f32[520,128]{1,0:T(8,128)S(1)} %get-tuple-element.18._.rows0), channel_id=1, source_target_pairs={{0,1},{1,0},{2,3},{3,2},{4,5},{5,4},{6,7},{7,6},{8,9},{9,8},{10,11... | collective-permute-start | bytes 798728 | tf_op jit(solution)/shard_map/ppermute | solution.py:258
  9.6 2.4 %collective-permute-start.4 = (bf16[128,1024]{1,0:T(8,128)(2,1)}, bf16[128,1024]{1,0:T(8,128)(2,1)S(1)}, u32[]{:S(2)}, u32[]{:S(2)}) collective-permute-start(bf16[128,1024]{1,0:T(8,128)(2,1)} %o_h.1), channel_id=1, source_target_pairs={{0,1},{1,0},{2,3},{3,2},{4,5},{5,4},{6,7},{7,6},{8,9},{9,8},{10,11... | collective-permute-start | bytes 786440 | tf_op jit(solution)/shard_map/ppermute | solution.py:258
  12.0 20.5 %copy-start = (bf16[1,1024,640]{2,1,0:T(8,128)(2,1)S(1)}, bf16[1,1024,640]{2,1,0:T(8,128)(2,1)}, u32[]{:S(2)}) copy-start(bf16[1,1024,640]{2,1,0:T(8,128)(2,1)} %g0.1) | copy-start | bytes 3932164
  12.0 20.5 %copy-start.1 = (bf16[1,1024,640]{2,1,0:T(8,128)(2,1)S(1)}, bf16[1,1024,640]{2,1,0:T(8,128)(2,1)}, u32[]{:S(2)}) copy-start(bf16[1,1024,640]{2,1,0:T(8,128)(2,1)} %u0.1) | copy-start | bytes 3932164
  12.0 20.5 %copy-start.2 = (bf16[1,640,1024]{2,1,0:T(8,128)(2,1)S(1)}, bf16[1,640,1024]{2,1,0:T(8,128)(2,1)}, u32[]{:S(2)}) copy-start(bf16[1,640,1024]{2,1,0:T(8,128)(2,1)} %d0.1) | copy-start | bytes 3932164
  12.8 3.4 %collective-permute-start.6 = (bf16[64,256]{1,0:T(8,128)(2,1)S(1)}, bf16[64,256]{1,0:T(8,128)(2,1)S(1)}, u32[]{:S(2)}, u32[]{:S(2)}) collective-permute-start(bf16[64,256]{1,0:T(8,128)(2,1)S(1)} %get-tuple-element.24), channel_id=1, source_target_pairs={{0,3},{1,2},{2,1},{3,0},{4,7},{5,6},{6,5},{7,4},{8,11},{9,10},{10,... | collective-permute-start | bytes 98312 | tf_op jit(solution)/shard_map/ppermute | solution.py:253

commit v3 on v2

--- a/solution.py
+++ b/solution.py
@@ -55,7 +55,7 @@
     for c in copies:
         c.start()
     ends = 2 * seqs
-    rows[ends:, :] = jnp.zeros((rows.shape[0] - ends, channels), F32)
+    rows[ends : ends + 8, :] = jnp.zeros((8, channels), F32)
     for c in copies[: len(held)]:
         c.wait()
     total = conv[0].astype(F32) * taps[0:1, :].astype(F32)
@@ -66,13 +66,12 @@
     rows[ends + 1 : ends + 2, :] = -LRU_SCALE * jnp.log1p(jnp.exp(-lam[...])).reshape(1, -1)
     heads, width = wr.shape[0], wr.shape[1]
     for i, w in enumerate((wr, wi)):
-        base = ends + 8 + i * channels
+        base = ends + 8 + i * width
         for h in range(heads):
-            at = slice(h * width, (h + 1) * width)
-            rows[base + h * width : base + (h + 1) * width, at] = w[h].astype(F32)
+            rows[base : base + width, h * width : (h + 1) * width] = w[h].astype(F32)
     for c in copies[len(held) :]:
         c.wait()
-    base = ends + 8 + 2 * channels
+    base = ends + 8 + 2 * width
     for i in range(tok.shape[1] // channels):
         at = slice(i * channels, (i + 1) * channels)
         rows[base + i * seqs : base + (i + 1) * seqs, :] = tok[:, at].astype(F32)
@@ -133,7 +132,17 @@
     me = tp_index()
     seqs, quarter = t0.shape
     channels = rows0.shape[1]
-    base = 2 * seqs + 8 + 2 * channels
+    base = rows0.shape[0] - seqs * (quarter // channels)
+    width = (base - 2 * seqs - 8) // 2
+    shape = (channels, channels)
+    inside = (
+        lax.broadcasted_iota(jnp.int32, shape, 0) // width
+        == lax.broadcasted_iota(jnp.int32, shape, 1) // width
+    )
+
+    def spread(maps):
+        return jnp.where(inside, jnp.concatenate([maps] * (channels // width), axis=0), 0.0).astype(BF16)
+
     t1 = jnp.concatenate([rows1[i : i + seqs, :] for i in range(base, rows1.shape[0], seqs)], axis=1)
     pieces = [t0[...].astype(F32), t1, t2[...].astype(F32), t3[...].astype(F32)]
     squares = sum(jnp.sum(p * p, axis=1, keepdims=True) for p in pieces)
@@ -150,8 +159,8 @@
         conv_out = rows[:seqs, :] + branch * rows[2 * seqs : 2 * seqs + 1, :]
         heads = conv_out.astype(BF16)
         maps = 2 * seqs + 8
-        recur = jax.nn.sigmoid(dot(heads, rows[maps : maps + channels, :].astype(BF16)))
-        inject = jax.nn.sigmoid(dot(heads, rows[maps + channels : maps + 2 * channels, :].astype(BF16)))
+        recur = jax.nn.sigmoid(dot(heads, spread(rows[maps : maps + width, :])))
+        inject = jax.nn.sigmoid(dot(heads, spread(rows[maps + width : base, :])))
         log_decay = recur * rows[2 * seqs + 1 : 2 * seqs + 2, :]
         y = -2.0 * log_decay
         series = y * (1.0 - y * (1 / 2) * (1.0 - y * (1 / 3) * (1.0 - y * (1 / 4) * (1.0 - y * (1 / 5)))))
@@ -269,10 +278,7 @@
     )
     rows_0, here = call(
         pack,
-        [
-            ((2 * seqs + 8 + 2 * channels + seqs * (quarter // channels), channels), F32),
-            (tokens.shape, BF16),
-        ],
+        [((2 * seqs + 8 + 2 * w_recur.shape[1] + seqs * (quarter // channels), channels), F32), (tokens.shape, BF16)],
         *mixing,
         far=len(mixing),
         scratch=[pltpu.VMEM(a.shape, a.dtype) for a in mixing[:5]]

time: 47.7 us -> 48.8 us (1.023)
  waiting for transfers between devices: 5.47 us -> 6.53 us
    ppermute x4, waiting for transfers between devices: 1.16 us -> 2.22 us  [beside(): return lax.ppermute(x, 'xb', SWAP)]
  transfers between devices with their start and end apart: 10 -> 10, of which waited for: 4 -> 5; matrix products, arithmetic and copies ran while one was open for 0% -> 0% of each run, Pallas kernels for 9% -> 8%
where the time goes in v3:
time: 48.8 us; the launch traced here: 48.5 us
  blocking collectives  28.7 us (59%)
  waiting for transfers between devices  6.53 us (13%)
  Pallas kernels  6.4 us (13%)
  starting transfers between devices  6.16 us (13%)
  between operations  0.72 us (1%)
    all_to_all x1, blocking collectives, step(): lax.all_to_all(sent, ring, split_axis=0, concat_axis=0, tiled=True)  16.1 us
    all_to_all x1, blocking collectives, step(): lax.all_to_all(term.reshape(na * slots, quarter), ring, split_axis=0, con...  12.6 us
    pallas_call x7, Pallas kernels, call(): pl.pallas_call(kernel, out_shape=[jax.ShapeDtypeStruct(s, d) if i in fina...  6.4 us
    ppermute x3, starting transfers between devices, swapped(): return lax.ppermute(x, tp, [(i, i ^ k) for i in range(n_tp)])  4.68 us
    ppermute x3, waiting for transfers between devices, swapped(): return lax.ppermute(x, tp, [(i, i ^ k) for i in range(n_tp)])  4.3 us
    ppermute x4, waiting for transfers between devices, beside(): return lax.ppermute(x, 'xb', SWAP)  2.22 us
    ppermute x4, starting transfers between devices, beside(): return lax.ppermute(x, 'xb', SWAP)  1.22 us
  transfers between devices with their start and end apart: 10, of which 5 were waited for; matrix products, arithmetic and copies ran while one was open for 0% of the time, Pallas kernels for 8%

profile of v3, /device:TPU:0, one launch (start us, length us, event | category | flops | bytes accessed | tf_op | source)
XLA Modules:
  0.0 48.5 jit_solution(6704124099992719872)
XLA Ops:
  0.6 0.6 %collective-permute-start.2 = (bf16[1024,128]{1,0:T(8,128)(2,1)}, bf16[1024,128]{1,0:T(8,128)(2,1)S(1)}, u32[]{:S(2)}, u32[]{:S(2)}) collective-permute-start(bf16[1024,128]{1,0:T(8,128)(2,1)} %b_h.1), channel_id=1, source_target_pairs={{0,1},{1,0},{2,3},{3,2},{4,5},{5,4},{6,7},{7,6},{8,9},{9,8},{10,11... | collective-permute-start | bytes 786440 | tf_op jit(solution)/shard_map/ppermute | solution.py:267
  1.2 1.0 %shard_map.176 = (f32[392,128]{1,0:T(8,128)S(1)}, bf16[64,256]{1,0:T(8,128)(2,1)S(1)}) custom-call(bf16[3,64,128]{2,1,0:T(8,128)(2,1)} %bitcast.11, bf16[4,128]{1,0:T(4,128)(2,1)} %taps_h.1, bf16[2,64,64]{2,1,0:T(8,128)(2,1)} %wr_h.1, bf16[2,64,64]{2,1,0:T(8,128)(2,1)} %wi_h.1, f32[128]{0:T(128)} %lam_h.1, f32[64,128]{1,0:T(8,128)} %state_h.1, ...), custom_call_target="tpu_custom_call" | custom-call | flops 100000 | tf_op jit(solution)/shard_map/pallas_call | solution.py:18
  2.2 0.1 collective-permute-start.5
  2.3 2.6 %collective-permute-start.1 = (bf16[64,256]{1,0:T(8,128)(2,1)}, bf16[64,256]{1,0:T(8,128)(2,1)S(1)}, u32[]{:S(2)}, u32[]{:S(2)}) collective-permute-start(bf16[64,256]{1,0:T(8,128)(2,1)} %tok_h.1), channel_id=1, source_target_pairs={{0,3},{1,2},{2,1},{3,0},{4,7},{5,6},{6,5},{7,4},{8,11},{9,10},{10,... | collective-permute-start | bytes 98312 | tf_op jit(solution)/shard_map/ppermute | solution.py:262
  4.9 0.3 collective-permute-start
  5.2 0.1 collective-permute-start.7
  5.3 1.7 %collective-permute-done.1.t3 = bf16[64,256]{1,0:T(8,128)(2,1)S(1)} collective-permute-done((bf16[64,256]{1,0:T(8,128)(2,1)}, bf16[64,256]{1,0:T(8,128)(2,1)S(1)}, u32[]{:S(2)}, u32[]{:S(2)}) %collective-permute-start.1) | collective-permute-done | bytes 32800 | tf_op jit(solution)/shard_map/ppermute | solution.py:262
  7.0 0.1 collective-permute-start.8
  7.1 1.9 %collective-permute-done.t2 = bf16[64,256]{1,0:T(8,128)(2,1)S(1)} collective-permute-done((bf16[64,256]{1,0:T(8,128)(2,1)}, bf16[64,256]{1,0:T(8,128)(2,1)S(1)}, u32[]{:S(2)}, u32[]{:S(2)}) %collective-permute-start) | collective-permute-done | bytes 32800 | tf_op jit(solution)/shard_map/ppermute | solution.py:262
  9.0 0.0 collective-permute-start.9
  9.0 0.0 collective-permute-done.5.rows1
  9.0 0.5 %collective-permute-start.3 = (bf16[1024,128]{1,0:T(8,128)(2,1)}, bf16[1024,128]{1,0:T(8,128)(2,1)S(1)}, u32[]{:S(2)}, u32[]{:S(2)}) collective-permute-start(bf16[1024,128]{1,0:T(8,128)(2,1)} %g_h.1), channel_id=1, source_target_pairs={{0,1},{1,0},{2,3},{3,2},{4,5},{5,4},{6,7},{7,6},{8,9},{9,8},{10,11... | collective-permute-start | bytes 786440 | tf_op jit(solution)/shard_map/ppermute | solution.py:267
  9.5 0.0 collective-permute-done.2.b1
  9.5 0.1 collective-permute-start.4
  9.6 1.2 %shard_map.177 = (f32[1,1024]{1,0:T(1,128)S(1)}, f32[1,1024]{1,0:T(1,128)S(1)}, bf16[1024,128]{1,0:T(8,128)(2,1)S(1)}, bf16[1024,128]{1,0:T(8,128)(2,1)S(1)}, bf16[128,1024]{1,0:T(8,128)(2,1)S(1)}) custom-call(bf16[1024]{0:T(1024)(128)(2,1)} %mix_h.1, bf16[1024]{0:T(1024)(128)(2,1)} %ffn_h.1, bf16[1024,128]{1,0:T(8,128)(2,1)} %b_h.1, bf16[1024,128]{1,0:T(8,128)(2,1)} %g_h.1, ...), custom_call_target="tpu_custom_call" | custom-call | flops 1000000 | tf_op jit(solution)/shard_map/pallas_call | solution.py:18
  10.8 1.8 %collective-permute-done.3.g1 = bf16[1024,128]{1,0:T(8,128)(2,1)S(1)} collective-permute-done((bf16[1024,128]{1,0:T(8,128)(2,1)}, bf16[1024,128]{1,0:T(8,128)(2,1)S(1)}, u32[]{:S(2)}, u32[]{:S(2)}) %collective-permute-start.3) | collective-permute-done | bytes 262176 | tf_op jit(solution)/shard_map/ppermute | solution.py:267
  12.7 0.4 collective-permute-done.4.out1
  13.0 0.0 copy-start
  13.0 0.0 copy-start.1
  13.0 0.0 copy-start.2
  13.0 0.7 %shard_map.178 = (f32[64,128]{1,0:T(8,128)S(1)}, f32[64,256]{1,0:T(8,128)S(1)}, bf16[64,256]{1,0:T(8,128)(2,1)S(1)}) custom-call(bf16[64,256]{1,0:T(8,128)(2,1)S(1)} %get-tuple-element.17.t0.tokens, bf16[64,256]{1,0:T(8,128)(2,1)S(1)} %collective-permute-done.t2, bf16[64,256]{1,0:T(8,128)(2,1)S(1)} %collective-permute-done.1.t3, ...), custom_call_target="tpu_custom_call" | custom-call | flops 5000000000 | tf_op jit(solution)/shard_map/pallas_call | solution.py:18
  13.8 1.7 %collective-permute-start.6 = (bf16[64,256]{1,0:T(8,128)(2,1)S(1)}, bf16[64,256]{1,0:T(8,128)(2,1)S(1)}, u32[]{:S(2)}, u32[]{:S(2)}) collective-permute-start(bf16[64,256]{1,0:T(8,128)(2,1)S(1)} %get-tuple-element.24), channel_id=1, source_target_pairs={{0,3},{1,2},{2,1},{3,0},{4,7},{5,6},{6,5},{7,4},{8,11},{9,10},{10,... | collective-permute-start | bytes 98312 | tf_op jit(solution)/shard_map/ppermute | solution.py:262
  15.5 1.0 %shard_map.179 = (bf16[256,64]{1,0:T(8,128)(2,1)S(1)}, bf16[128,256]{1,0:T(8,128)(2,1)S(1)}, f32[2,64,128]{2,1,0:T(8,128)S(1)}) custom-call(s32[2,64]{1,0:T(2,128)} %bitcast.12, f32[2,64]{1,0:T(2,128)} %bitcast.13, f32[64,256]{1,0:T(8,128)S(1)} %get-tuple-element.23._.keep), custom_call_target="tpu_custom_call" | custom-call | flops 1000000 | tf_op jit(solution)/shard_map/pallas_call | solution.py:18
  16.5 0.7 %collective-permute-done.6.other = bf16[64,256]{1,0:T(8,128)(2,1)S(1)} collective-permute-done((bf16[64,256]{1,0:T(8,128)(2,1)S(1)}, bf16[64,256]{1,0:T(8,128)(2,1)S(1)}, u32[]{:S(2)}, u32[]{:S(2)}) %collective-permute-start.6) | collective-permute-done | bytes 32800 | tf_op jit(solution)/shard_map/ppermute | solution.py:262
  17.2 0.2 shard_map.180
  17.4 16.1 %all_to_all.20 = bf16[32,16,256]{2,1,0:T(8,128)(2,1)S(1)} all-to-all(bf16[32,16,256]{2,1,0:T(8,128)(2,1)S(1)} %bitcast.10), channel_id=1, replica_groups=mesh['ep'=8,'xa'=2,'xb'=2] {'xa','ep','xb'}, dimensions={0} | all-to-all | bytes 524288 | tf_op jit(solution)/shard_map/all_to_all | solution.py:341
  33.5 0.0 collective-permute-done.7.g1
  33.5 0.0 collective-permute-done.8.u1
  33.5 0.0 collective-permute-done.9.d1
  33.5 0.0 copy-done
  33.5 0.0 copy-done.1
  33.5 0.0 copy-done.2
  33.5 1.5 %shard_map.181 = bf16[2,8,32,256]{3,2,1,0:T(8,128)(2,1)S(1)} custom-call(bf16[2,8,32,256]{3,2,1,0:T(8,128)(2,1)S(1)} %bitcast.8, f32[1,1024]{1,0:T(1,128)S(1)} %get-tuple-element.28.ffn_row, bf16[1,1024,640]{2,1,0:T(8,128)(2,1)S(1)} %copy-done, bf16[1,1024,640]{2,1,0:T(8,128)(2,1)S(1)} %copy-done.1, bf16[1,640,1024]{2,1,0:T(8,128)(2,1)S(1)} %copy-done.2, ...), custom_call_target="tpu_custom_call" | custom-call | flops 1000000000 | tf_op jit(solution)/shard_map/pallas_call | solution.py:18
  35.1 12.6 %all_to_all.21 = bf16[32,16,256]{2,1,0:T(8,128)(2,1)S(1)} all-to-all(bf16[32,16,256]{2,1,0:T(8,128)(2,1)S(1)} %bitcast.9), channel_id=1, replica_groups=mesh['ep'=8,'xa'=2,'xb'=2] {'xa','ep','xb'}, dimensions={0} | all-to-all | bytes 524288 | tf_op jit(solution)/shard_map/all_to_all | solution.py:355
  47.7 0.9 %shard_map.182 = (bf16[64,256]{1,0:T(8,128)(2,1)}, f32[64,128]{1,0:T(8,128)}) custom-call(bf16[64,256]{1,0:T(8,128)(2,1)S(1)} %get-tuple-element.26.resid, bf16[512,256]{1,0:T(8,128)(2,1)S(1)} %bitcast.7, bf16[128,256]{1,0:T(8,128)(2,1)S(1)} %get-tuple-element.29.hits, f32[2,64,128]{2,1,0:T(8,128)S(1)} %get-tuple-element.30.wcol, ...), custom_call_target="tpu_custom_call" | custom-call | tf_op jit(solution)/shard_map/pallas_call | solution.py:18
Async XLA Ops:
  0.6 8.9 %collective-permute-start.2 = (bf16[1024,128]{1,0:T(8,128)(2,1)}, bf16[1024,128]{1,0:T(8,128)(2,1)S(1)}, u32[]{:S(2)}, u32[]{:S(2)}) collective-permute-start(bf16[1024,128]{1,0:T(8,128)(2,1)} %b_h.1), channel_id=1, source_target_pairs={{0,1},{1,0},{2,3},{3,2},{4,5},{5,4},{6,7},{7,6},{8,9},{9,8},{10,11... | collective-permute-start | bytes 786440 | tf_op jit(solution)/shard_map/ppermute | solution.py:267
  2.2 6.9 %collective-permute-start.5 = (f32[392,128]{1,0:T(8,128)S(1)}, f32[392,128]{1,0:T(8,128)S(1)}, u32[]{:S(2)}, u32[]{:S(2)}) collective-permute-start(f32[392,128]{1,0:T(8,128)S(1)} %get-tuple-element.18._.rows0), channel_id=1, source_target_pairs={{0,1},{1,0},{2,3},{3,2},{4,5},{5,4},{6,7},{7,6},{8,9},{9,8},{10,11... | collective-permute-start | bytes 602120 | tf_op jit(solution)/shard_map/ppermute | solution.py:267
  2.3 4.8 %collective-permute-start.1 = (bf16[64,256]{1,0:T(8,128)(2,1)}, bf16[64,256]{1,0:T(8,128)(2,1)S(1)}, u32[]{:S(2)}, u32[]{:S(2)}) collective-permute-start(bf16[64,256]{1,0:T(8,128)(2,1)} %tok_h.1), channel_id=1, source_target_pairs={{0,3},{1,2},{2,1},{3,0},{4,7},{5,6},{6,5},{7,4},{8,11},{9,10},{10,... | collective-permute-start | bytes 98312 | tf_op jit(solution)/shard_map/ppermute | solution.py:262
  4.9 4.1 %collective-permute-start = (bf16[64,256]{1,0:T(8,128)(2,1)}, bf16[64,256]{1,0:T(8,128)(2,1)S(1)}, u32[]{:S(2)}, u32[]{:S(2)}) collective-permute-start(bf16[64,256]{1,0:T(8,128)(2,1)} %tok_h.1), channel_id=1, source_target_pairs={{0,2},{1,3},{2,0},{3,1},{4,6},{5,7},{6,4},{7,5},{8,10},{9,11},{10,... | collective-permute-start | bytes 98312 | tf_op jit(solution)/shard_map/ppermute | solution.py:262
  5.2 28.3 %collective-permute-start.7 = (bf16[1,1024,640]{2,1,0:T(8,128)(2,1)}, bf16[1,1024,640]{2,1,0:T(8,128)(2,1)S(1)}, u32[]{:S(2)}, u32[]{:S(2)}) collective-permute-start(bf16[1,1024,640]{2,1,0:T(8,128)(2,1)} %g0.1), channel_id=1, source_target_pairs={{0,1},{1,0},{2,3},{3,2},{4,5},{5,4},{6,7},{7,6},{8,9},{9,8},{10,11... | collective-permute-start | bytes 3932168 | tf_op jit(solution)/shard_map/ppermute | solution.py:339
  7.0 26.5 %collective-permute-start.8 = (bf16[1,1024,640]{2,1,0:T(8,128)(2,1)}, bf16[1,1024,640]{2,1,0:T(8,128)(2,1)S(1)}, u32[]{:S(2)}, u32[]{:S(2)}) collective-permute-start(bf16[1,1024,640]{2,1,0:T(8,128)(2,1)} %u0.1), channel_id=1, source_target_pairs={{0,1},{1,0},{2,3},{3,2},{4,5},{5,4},{6,7},{7,6},{8,9},{9,8},{10,11... | collective-permute-start | bytes 3932168 | tf_op jit(solution)/shard_map/ppermute | solution.py:339
  9.0 24.5 %collective-permute-start.9 = (bf16[1,640,1024]{2,1,0:T(8,128)(2,1)}, bf16[1,640,1024]{2,1,0:T(8,128)(2,1)S(1)}, u32[]{:S(2)}, u32[]{:S(2)}) collective-permute-start(bf16[1,640,1024]{2,1,0:T(8,128)(2,1)} %d0.1), channel_id=1, source_target_pairs={{0,1},{1,0},{2,3},{3,2},{4,5},{5,4},{6,7},{7,6},{8,9},{9,8},{10,11... | collective-permute-start | bytes 3932168 | tf_op jit(solution)/shard_map/ppermute | solution.py:339
  9.0 3.6 %collective-permute-start.3 = (bf16[1024,128]{1,0:T(8,128)(2,1)}, bf16[1024,128]{1,0:T(8,128)(2,1)S(1)}, u32[]{:S(2)}, u32[]{:S(2)}) collective-permute-start(bf16[1024,128]{1,0:T(8,128)(2,1)} %g_h.1), channel_id=1, source_target_pairs={{0,1},{1,0},{2,3},{3,2},{4,5},{5,4},{6,7},{7,6},{8,9},{9,8},{10,11... | collective-permute-start | bytes 786440 | tf_op jit(solution)/shard_map/ppermute | solution.py:267
  9.5 3.5 %collective-permute-start.4 = (bf16[128,1024]{1,0:T(8,128)(2,1)}, bf16[128,1024]{1,0:T(8,128)(2,1)S(1)}, u32[]{:S(2)}, u32[]{:S(2)}) collective-permute-start(bf16[128,1024]{1,0:T(8,128)(2,1)} %o_h.1), channel_id=1, source_target_pairs={{0,1},{1,0},{2,3},{3,2},{4,5},{5,4},{6,7},{7,6},{8,9},{9,8},{10,11... | collective-permute-start | bytes 786440 | tf_op jit(solution)/shard_map/ppermute | solution.py:267
  13.0 20.5 %copy-start = (bf16[1,1024,640]{2,1,0:T(8,128)(2,1)S(1)}, bf16[1,1024,640]{2,1,0:T(8,128)(2,1)}, u32[]{:S(2)}) copy-start(bf16[1,1024,640]{2,1,0:T(8,128)(2,1)} %g0.1) | copy-start | bytes 3932164
  13.0 20.5 %copy-start.1 = (bf16[1,1024,640]{2,1,0:T(8,128)(2,1)S(1)}, bf16[1,1024,640]{2,1,0:T(8,128)(2,1)}, u32[]{:S(2)}) copy-start(bf16[1,1024,640]{2,1,0:T(8,128)(2,1)} %u0.1) | copy-start | bytes 3932164
  13.0 20.5 %copy-start.2 = (bf16[1,640,1024]{2,1,0:T(8,128)(2,1)S(1)}, bf16[1,640,1024]{2,1,0:T(8,128)(2,1)}, u32[]{:S(2)}) copy-start(bf16[1,640,1024]{2,1,0:T(8,128)(2,1)} %d0.1) | copy-start | bytes 3932164
  13.8 3.4 %collective-permute-start.6 = (bf16[64,256]{1,0:T(8,128)(2,1)S(1)}, bf16[64,256]{1,0:T(8,128)(2,1)S(1)}, u32[]{:S(2)}, u32[]{:S(2)}) collective-permute-start(bf16[64,256]{1,0:T(8,128)(2,1)S(1)} %get-tuple-element.24), channel_id=1, source_target_pairs={{0,3},{1,2},{2,1},{3,0},{4,7},{5,6},{6,5},{7,4},{8,11},{9,10},{10,... | collective-permute-start | bytes 98312 | tf_op jit(solution)/shard_map/ppermute | solution.py:262

commit v4 on v3

--- a/solution.py
+++ b/solution.py
@@ -185,7 +185,9 @@
         sent[a : a + slots, :] = buffer
 
 
-def experts_of(got, ffn_row, g0, u0, d0, g1, u1, d1, out, rows):
+def experts_of(got, ffn_row, g0, u0, d0, g1, u1, d1, state, out, state_h, rows, sem):
+    leaving = pltpu.make_async_copy(state, state_h, sem)
+    leaving.start()
     na, sources, both, quarter = got.shape
     nb = rows.shape[1] // (na * quarter)
     half = both // nb
@@ -205,11 +207,11 @@
         at = slice(t * quarter, (t + 1) * quarter)
         term = dot(hidden[0], d0[0, :, at]) + dot(hidden[1], d1[0, :, at])
         out[x, :, part, :] = term.astype(BF16).reshape(sources, half, quarter)
-
-
-def combine(resid, back, hits, wcol, state, mixed_h, state_h, mixed, sem):
-    leaving = [pltpu.make_async_copy(state, state_h, sem.at[0])]
-    leaving[0].start()
+    leaving.wait()
+
+
+def combine(resid, back, hits, wcol, mixed_h, mixed, sem):
+    leaving = []
     top, seqs, width = wcol.shape
     slots = hits.shape[1]
     for j, i in enumerate(range(0, resid.shape[1], width)):
@@ -219,7 +221,7 @@
         for k in range(top):
             total = total + picked[k * seqs : (k + 1) * seqs, :] * wcol[k]
         mixed[:, at] = total.astype(BF16)
-        leaving.append(pltpu.make_async_copy(mixed.at[:, at], mixed_h.at[:, at], sem.at[j + 1]))
+        leaving.append(pltpu.make_async_copy(mixed.at[:, at], mixed_h.at[:, at], sem.at[j]))
         leaving[-1].start()
     for c in leaving:
         c.wait()
@@ -339,31 +341,33 @@
         partners.append(lax.ppermute(w, "xb", SWAP))
     blocks = (na, experts, nb * half, quarter)
     arrived = lax.all_to_all(sent, ring, split_axis=0, concat_axis=0, tiled=True)
-    (term,) = call(
+    term, state_out = call(
         experts_of,
-        [(blocks, BF16)],
+        [(blocks, BF16), ((seqs, channels), F32)],
         arrived.reshape(blocks),
         ffn_row,
         expert_gate,
         expert_up,
         expert_down,
         *partners,
-        scratch=[pltpu.VMEM((slots // nb, features), BF16)],
+        state,
+        final=(1,),
+        scratch=[pltpu.VMEM((slots // nb, features), BF16), pltpu.SemaphoreType.DMA],
         flops=10**9,
         limit=8 << 20,
     )
     back = lax.all_to_all(term.reshape(na * slots, quarter), ring, split_axis=0, concat_axis=0, tiled=True)
-    return call(
+    (mixed,) = call(
         combine,
-        [((seqs, quarter), BF16), ((seqs, channels), F32)],
+        [((seqs, quarter), BF16)],
         resid,
         back,
         hits,
         wcol,
-        state,
-        final=(0, 1),
-        scratch=[pltpu.VMEM((seqs, quarter), BF16), pltpu.SemaphoreType.DMA((1 + quarter // 128,))],
-    )
+        final=(0,),
+        scratch=[pltpu.VMEM((seqs, quarter), BF16), pltpu.SemaphoreType.DMA((quarter // 128,))],
+    )
+    return (mixed, state_out)
 
 
 def solution(mesh):

time: 48.8 us -> 48.8 us (level)
  no operation moved by 1% of the time
where the time goes in v4:
time: 48.8 us; the launch traced here: 48.5 us
  blocking collectives  28.7 us (59%)
  waiting for transfers between devices  6.53 us (13%)
  Pallas kernels  6.41 us (13%)
  starting transfers between devices  6.16 us (13%)
  between operations  0.72 us (1%)
    all_to_all x1, blocking collectives, step(): lax.all_to_all(sent, ring, split_axis=0, concat_axis=0, tiled=True)  16.1 us
    all_to_all x1, blocking collectives, step(): lax.all_to_all(term.reshape(na * slots, quarter), ring, split_axis=0, con...  12.6 us
    pallas_call x7, Pallas kernels, call(): pl.pallas_call(kernel, out_shape=[jax.ShapeDtypeStruct(s, d) if i in fina...  6.41 us
    ppermute x3, starting transfers between devices, swapped(): return lax.ppermute(x, tp, [(i, i ^ k) for i in range(n_tp)])  4.68 us
    ppermute x3, waiting for transfers between devices, swapped(): return lax.ppermute(x, tp, [(i, i ^ k) for i in range(n_tp)])  4.3 us
    ppermute x4, waiting for transfers between devices, beside(): return lax.ppermute(x, 'xb', SWAP)  2.22 us
    ppermute x4, starting transfers between devices, beside(): return lax.ppermute(x, 'xb', SWAP)  1.22 us
  transfers between devices with their start and end apart: 10, of which 5 were waited for; matrix products, arithmetic and copies ran while one was open for 0% of the time, Pallas kernels for 8%

profile of v4, /device:TPU:0, one launch (start us, length us, event | category | flops | bytes accessed | tf_op | source)
XLA Modules:
  0.0 48.5 jit_solution(1559288796197712365)
XLA Ops:
  0.6 0.6 %collective-permute-start.2 = (bf16[1024,128]{1,0:T(8,128)(2,1)}, bf16[1024,128]{1,0:T(8,128)(2,1)S(1)}, u32[]{:S(2)}, u32[]{:S(2)}) collective-permute-start(bf16[1024,128]{1,0:T(8,128)(2,1)} %b_h.1), channel_id=1, source_target_pairs={{0,1},{1,0},{2,3},{3,2},{4,5},{5,4},{6,7},{7,6},{8,9},{9,8},{10,11... | collective-permute-start | bytes 786440 | tf_op jit(solution)/shard_map/ppermute | solution.py:269
  1.2 1.0 %shard_map.176 = (f32[392,128]{1,0:T(8,128)S(1)}, bf16[64,256]{1,0:T(8,128)(2,1)S(1)}) custom-call(bf16[3,64,128]{2,1,0:T(8,128)(2,1)} %bitcast.11, bf16[4,128]{1,0:T(4,128)(2,1)} %taps_h.1, bf16[2,64,64]{2,1,0:T(8,128)(2,1)} %wr_h.1, bf16[2,64,64]{2,1,0:T(8,128)(2,1)} %wi_h.1, f32[128]{0:T(128)} %lam_h.1, f32[64,128]{1,0:T(8,128)} %state_h.1, ...), custom_call_target="tpu_custom_call" | custom-call | flops 100000 | tf_op jit(solution)/shard_map/pallas_call | solution.py:18
  2.2 0.1 collective-permute-start.5
  2.3 2.6 %collective-permute-start.1 = (bf16[64,256]{1,0:T(8,128)(2,1)}, bf16[64,256]{1,0:T(8,128)(2,1)S(1)}, u32[]{:S(2)}, u32[]{:S(2)}) collective-permute-start(bf16[64,256]{1,0:T(8,128)(2,1)} %tok_h.1), channel_id=1, source_target_pairs={{0,3},{1,2},{2,1},{3,0},{4,7},{5,6},{6,5},{7,4},{8,11},{9,10},{10,... | collective-permute-start | bytes 98312 | tf_op jit(solution)/shard_map/ppermute | solution.py:264
  4.9 0.3 collective-permute-start
  5.2 0.1 collective-permute-start.7
  5.3 1.7 %collective-permute-done.1.t3 = bf16[64,256]{1,0:T(8,128)(2,1)S(1)} collective-permute-done((bf16[64,256]{1,0:T(8,128)(2,1)}, bf16[64,256]{1,0:T(8,128)(2,1)S(1)}, u32[]{:S(2)}, u32[]{:S(2)}) %collective-permute-start.1) | collective-permute-done | bytes 32800 | tf_op jit(solution)/shard_map/ppermute | solution.py:264
  7.0 0.1 collective-permute-start.8
  7.1 1.9 %collective-permute-done.t2 = bf16[64,256]{1,0:T(8,128)(2,1)S(1)} collective-permute-done((bf16[64,256]{1,0:T(8,128)(2,1)}, bf16[64,256]{1,0:T(8,128)(2,1)S(1)}, u32[]{:S(2)}, u32[]{:S(2)}) %collective-permute-start) | collective-permute-done | bytes 32800 | tf_op jit(solution)/shard_map/ppermute | solution.py:264
  9.0 0.0 collective-permute-start.9
  9.0 0.0 collective-permute-done.5.rows1
  9.0 0.5 %collective-permute-start.3 = (bf16[1024,128]{1,0:T(8,128)(2,1)}, bf16[1024,128]{1,0:T(8,128)(2,1)S(1)}, u32[]{:S(2)}, u32[]{:S(2)}) collective-permute-start(bf16[1024,128]{1,0:T(8,128)(2,1)} %g_h.1), channel_id=1, source_target_pairs={{0,1},{1,0},{2,3},{3,2},{4,5},{5,4},{6,7},{7,6},{8,9},{9,8},{10,11... | collective-permute-start | bytes 786440 | tf_op jit(solution)/shard_map/ppermute | solution.py:269
  9.5 0.0 collective-permute-done.2.b1
  9.5 0.1 collective-permute-start.4
  9.6 1.2 %shard_map.177 = (f32[1,1024]{1,0:T(1,128)S(1)}, f32[1,1024]{1,0:T(1,128)S(1)}, bf16[1024,128]{1,0:T(8,128)(2,1)S(1)}, bf16[1024,128]{1,0:T(8,128)(2,1)S(1)}, bf16[128,1024]{1,0:T(8,128)(2,1)S(1)}) custom-call(bf16[1024]{0:T(1024)(128)(2,1)} %mix_h.1, bf16[1024]{0:T(1024)(128)(2,1)} %ffn_h.1, bf16[1024,128]{1,0:T(8,128)(2,1)} %b_h.1, bf16[1024,128]{1,0:T(8,128)(2,1)} %g_h.1, ...), custom_call_target="tpu_custom_call" | custom-call | flops 1000000 | tf_op jit(solution)/shard_map/pallas_call | solution.py:18
  10.8 1.8 %collective-permute-done.3.g1 = bf16[1024,128]{1,0:T(8,128)(2,1)S(1)} collective-permute-done((bf16[1024,128]{1,0:T(8,128)(2,1)}, bf16[1024,128]{1,0:T(8,128)(2,1)S(1)}, u32[]{:S(2)}, u32[]{:S(2)}) %collective-permute-start.3) | collective-permute-done | bytes 262176 | tf_op jit(solution)/shard_map/ppermute | solution.py:269
  12.7 0.4 collective-permute-done.4.out1
  13.0 0.0 copy-start
  13.0 0.0 copy-start.1
  13.0 0.0 copy-start.2
  13.0 0.7 %shard_map.178 = (f32[64,128]{1,0:T(8,128)S(1)}, f32[64,256]{1,0:T(8,128)S(1)}, bf16[64,256]{1,0:T(8,128)(2,1)S(1)}) custom-call(bf16[64,256]{1,0:T(8,128)(2,1)S(1)} %get-tuple-element.19.t0.tokens, bf16[64,256]{1,0:T(8,128)(2,1)S(1)} %collective-permute-done.t2, bf16[64,256]{1,0:T(8,128)(2,1)S(1)} %collective-permute-done.1.t3, ...), custom_call_target="tpu_custom_call" | custom-call | flops 5000000000 | tf_op jit(solution)/shard_map/pallas_call | solution.py:18
  13.8 1.7 %collective-permute-start.6 = (bf16[64,256]{1,0:T(8,128)(2,1)S(1)}, bf16[64,256]{1,0:T(8,128)(2,1)S(1)}, u32[]{:S(2)}, u32[]{:S(2)}) collective-permute-start(bf16[64,256]{1,0:T(8,128)(2,1)S(1)} %get-tuple-element.26), channel_id=1, source_target_pairs={{0,3},{1,2},{2,1},{3,0},{4,7},{5,6},{6,5},{7,4},{8,11},{9,10},{10,... | collective-permute-start | bytes 98312 | tf_op jit(solution)/shard_map/ppermute | solution.py:264
  15.5 1.0 %shard_map.179 = (bf16[256,64]{1,0:T(8,128)(2,1)S(1)}, bf16[128,256]{1,0:T(8,128)(2,1)S(1)}, f32[2,64,128]{2,1,0:T(8,128)S(1)}) custom-call(s32[2,64]{1,0:T(2,128)} %bitcast.12, f32[2,64]{1,0:T(2,128)} %bitcast.13, f32[64,256]{1,0:T(8,128)S(1)} %get-tuple-element.25._.keep), custom_call_target="tpu_custom_call" | custom-call | flops 1000000 | tf_op jit(solution)/shard_map/pallas_call | solution.py:18
  16.5 0.7 %collective-permute-done.6.other = bf16[64,256]{1,0:T(8,128)(2,1)S(1)} collective-permute-done((bf16[64,256]{1,0:T(8,128)(2,1)S(1)}, bf16[64,256]{1,0:T(8,128)(2,1)S(1)}, u32[]{:S(2)}, u32[]{:S(2)}) %collective-permute-start.6) | collective-permute-done | bytes 32800 | tf_op jit(solution)/shard_map/ppermute | solution.py:264
  17.2 0.2 shard_map.180
  17.4 16.1 %all_to_all.20 = bf16[32,16,256]{2,1,0:T(8,128)(2,1)S(1)} all-to-all(bf16[32,16,256]{2,1,0:T(8,128)(2,1)S(1)} %bitcast.10), channel_id=1, replica_groups=mesh['ep'=8,'xa'=2,'xb'=2] {'xa','ep','xb'}, dimensions={0} | all-to-all | bytes 524288 | tf_op jit(solution)/shard_map/all_to_all | solution.py:343
  33.5 0.0 collective-permute-done.7.g1
  33.5 0.0 collective-permute-done.8.u1
  33.5 0.0 collective-permute-done.9.d1
  33.5 0.0 copy-done
  33.5 0.0 copy-done.1
  33.5 0.0 copy-done.2
  33.5 1.5 %shard_map.181 = (bf16[2,8,32,256]{3,2,1,0:T(8,128)(2,1)S(1)}, f32[64,128]{1,0:T(8,128)}) custom-call(bf16[2,8,32,256]{3,2,1,0:T(8,128)(2,1)S(1)} %bitcast.7, f32[1,1024]{1,0:T(1,128)S(1)} %get-tuple-element.30.ffn_row, bf16[1,1024,640]{2,1,0:T(8,128)(2,1)S(1)} %copy-done, bf16[1,1024,640]{2,1,0:T(8,128)(2,1)S(1)} %copy-done.1, ...), custom_call_target="tpu_custom_call" | custom-call | flops 1000000000 | tf_op jit(solution)/shard_map/pallas_call | solution.py:18
  35.1 12.6 %all_to_all.21 = bf16[32,16,256]{2,1,0:T(8,128)(2,1)S(1)} all-to-all(bf16[32,16,256]{2,1,0:T(8,128)(2,1)S(1)} %bitcast.9), channel_id=1, replica_groups=mesh['ep'=8,'xa'=2,'xb'=2] {'xa','ep','xb'}, dimensions={0} | all-to-all | bytes 524288 | tf_op jit(solution)/shard_map/all_to_all | solution.py:359
  47.7 0.8 %shard_map.182 = bf16[64,256]{1,0:T(8,128)(2,1)} custom-call(bf16[64,256]{1,0:T(8,128)(2,1)S(1)} %get-tuple-element.28.resid, bf16[512,256]{1,0:T(8,128)(2,1)S(1)} %bitcast.8, bf16[128,256]{1,0:T(8,128)(2,1)S(1)} %get-tuple-element.33.hits, f32[2,64,128]{2,1,0:T(8,128)S(1)} %get-tuple-element.34.wcol), custom_call_target="tpu_custom_call" | custom-call | tf_op jit(solution)/shard_map/pallas_call | solution.py:18
Async XLA Ops:
  0.6 8.9 %collective-permute-start.2 = (bf16[1024,128]{1,0:T(8,128)(2,1)}, bf16[1024,128]{1,0:T(8,128)(2,1)S(1)}, u32[]{:S(2)}, u32[]{:S(2)}) collective-permute-start(bf16[1024,128]{1,0:T(8,128)(2,1)} %b_h.1), channel_id=1, source_target_pairs={{0,1},{1,0},{2,3},{3,2},{4,5},{5,4},{6,7},{7,6},{8,9},{9,8},{10,11... | collective-permute-start | bytes 786440 | tf_op jit(solution)/shard_map/ppermute | solution.py:269
  2.2 6.9 %collective-permute-start.5 = (f32[392,128]{1,0:T(8,128)S(1)}, f32[392,128]{1,0:T(8,128)S(1)}, u32[]{:S(2)}, u32[]{:S(2)}) collective-permute-start(f32[392,128]{1,0:T(8,128)S(1)} %get-tuple-element.20._.rows0), channel_id=1, source_target_pairs={{0,1},{1,0},{2,3},{3,2},{4,5},{5,4},{6,7},{7,6},{8,9},{9,8},{10,11... | collective-permute-start | bytes 602120 | tf_op jit(solution)/shard_map/ppermute | solution.py:269
  2.3 4.8 %collective-permute-start.1 = (bf16[64,256]{1,0:T(8,128)(2,1)}, bf16[64,256]{1,0:T(8,128)(2,1)S(1)}, u32[]{:S(2)}, u32[]{:S(2)}) collective-permute-start(bf16[64,256]{1,0:T(8,128)(2,1)} %tok_h.1), channel_id=1, source_target_pairs={{0,3},{1,2},{2,1},{3,0},{4,7},{5,6},{6,5},{7,4},{8,11},{9,10},{10,... | collective-permute-start | bytes 98312 | tf_op jit(solution)/shard_map/ppermute | solution.py:264
  4.9 4.1 %collective-permute-start = (bf16[64,256]{1,0:T(8,128)(2,1)}, bf16[64,256]{1,0:T(8,128)(2,1)S(1)}, u32[]{:S(2)}, u32[]{:S(2)}) collective-permute-start(bf16[64,256]{1,0:T(8,128)(2,1)} %tok_h.1), channel_id=1, source_target_pairs={{0,2},{1,3},{2,0},{3,1},{4,6},{5,7},{6,4},{7,5},{8,10},{9,11},{10,... | collective-permute-start | bytes 98312 | tf_op jit(solution)/shard_map/ppermute | solution.py:264
  5.2 28.3 %collective-permute-start.7 = (bf16[1,1024,640]{2,1,0:T(8,128)(2,1)}, bf16[1,1024,640]{2,1,0:T(8,128)(2,1)S(1)}, u32[]{:S(2)}, u32[]{:S(2)}) collective-permute-start(bf16[1,1024,640]{2,1,0:T(8,128)(2,1)} %g0.1), channel_id=1, source_target_pairs={{0,1},{1,0},{2,3},{3,2},{4,5},{5,4},{6,7},{7,6},{8,9},{9,8},{10,11... | collective-permute-start | bytes 3932168 | tf_op jit(solution)/shard_map/ppermute | solution.py:341
  7.0 26.5 %collective-permute-start.8 = (bf16[1,1024,640]{2,1,0:T(8,128)(2,1)}, bf16[1,1024,640]{2,1,0:T(8,128)(2,1)S(1)}, u32[]{:S(2)}, u32[]{:S(2)}) collective-permute-start(bf16[1,1024,640]{2,1,0:T(8,128)(2,1)} %u0.1), channel_id=1, source_target_pairs={{0,1},{1,0},{2,3},{3,2},{4,5},{5,4},{6,7},{7,6},{8,9},{9,8},{10,11... | collective-permute-start | bytes 3932168 | tf_op jit(solution)/shard_map/ppermute | solution.py:341
  9.0 24.5 %collective-permute-start.9 = (bf16[1,640,1024]{2,1,0:T(8,128)(2,1)}, bf16[1,640,1024]{2,1,0:T(8,128)(2,1)S(1)}, u32[]{:S(2)}, u32[]{:S(2)}) collective-permute-start(bf16[1,640,1024]{2,1,0:T(8,128)(2,1)} %d0.1), channel_id=1, source_target_pairs={{0,1},{1,0},{2,3},{3,2},{4,5},{5,4},{6,7},{7,6},{8,9},{9,8},{10,11... | collective-permute-start | bytes 3932168 | tf_op jit(solution)/shard_map/ppermute | solution.py:341
  9.0 3.6 %collective-permute-start.3 = (bf16[1024,128]{1,0:T(8,128)(2,1)}, bf16[1024,128]{1,0:T(8,128)(2,1)S(1)}, u32[]{:S(2)}, u32[]{:S(2)}) collective-permute-start(bf16[1024,128]{1,0:T(8,128)(2,1)} %g_h.1), channel_id=1, source_target_pairs={{0,1},{1,0},{2,3},{3,2},{4,5},{5,4},{6,7},{7,6},{8,9},{9,8},{10,11... | collective-permute-start | bytes 786440 | tf_op jit(solution)/shard_map/ppermute | solution.py:269
  9.5 3.5 %collective-permute-start.4 = (bf16[128,1024]{1,0:T(8,128)(2,1)}, bf16[128,1024]{1,0:T(8,128)(2,1)S(1)}, u32[]{:S(2)}, u32[]{:S(2)}) collective-permute-start(bf16[128,1024]{1,0:T(8,128)(2,1)} %o_h.1), channel_id=1, source_target_pairs={{0,1},{1,0},{2,3},{3,2},{4,5},{5,4},{6,7},{7,6},{8,9},{9,8},{10,11... | collective-permute-start | bytes 786440 | tf_op jit(solution)/shard_map/ppermute | solution.py:269
  13.0 20.5 %copy-start = (bf16[1,1024,640]{2,1,0:T(8,128)(2,1)S(1)}, bf16[1,1024,640]{2,1,0:T(8,128)(2,1)}, u32[]{:S(2)}) copy-start(bf16[1,1024,640]{2,1,0:T(8,128)(2,1)} %g0.1) | copy-start | bytes 3932164
  13.0 20.5 %copy-start.1 = (bf16[1,1024,640]{2,1,0:T(8,128)(2,1)S(1)}, bf16[1,1024,640]{2,1,0:T(8,128)(2,1)}, u32[]{:S(2)}) copy-start(bf16[1,1024,640]{2,1,0:T(8,128)(2,1)} %u0.1) | copy-start | bytes 3932164
  13.0 20.5 %copy-start.2 = (bf16[1,640,1024]{2,1,0:T(8,128)(2,1)S(1)}, bf16[1,640,1024]{2,1,0:T(8,128)(2,1)}, u32[]{:S(2)}) copy-start(bf16[1,640,1024]{2,1,0:T(8,128)(2,1)} %d0.1) | copy-start | bytes 3932164
  13.8 3.4 %collective-permute-start.6 = (bf16[64,256]{1,0:T(8,128)(2,1)S(1)}, bf16[64,256]{1,0:T(8,128)(2,1)S(1)}, u32[]{:S(2)}, u32[]{:S(2)}) collective-permute-start(bf16[64,256]{1,0:T(8,128)(2,1)S(1)} %get-tuple-element.26), channel_id=1, source_target_pairs={{0,3},{1,2},{2,1},{3,0},{4,7},{5,6},{6,5},{7,4},{8,11},{9,10},{10,... | collective-permute-start | bytes 98312 | tf_op jit(solution)/shard_map/ppermute | solution.py:264
